TPU v7x, 128 devices: a whole 4x4x4 slice. The times are simulated.
128 devices in a mesh: sp: 32 (over z, y, core), tp: 4 (over x).
Axes of the slice: x: 4, y: 4, z: 4, core: 2. Of those that a mesh axis runs over, the one named last changes fastest.
Arguments:
- tokens: bfloat16 [4096, 6, 2048], P(('sp', 'tp')), may hold values from -6 to 6
- norm_gain: float32 [2048], replicated, may hold values from 0.1 to 1.9
- w_query: bfloat16 [3, 2048, 1024], P(None, 'sp', 'tp'), may hold values from -0.125 to 0.125
- w_key: bfloat16 [3, 2048, 1024], P(None, 'sp', 'tp'), may hold values from -0.125 to 0.125
- w_value: bfloat16 [3, 2048, 1024], P(None, 'sp', 'tp'), may hold values from -0.125 to 0.125
- w_out: bfloat16 [1024, 2048], P('tp', 'sp'), may hold values from -0.1875 to 0.1875
Outputs:
- mixed: bfloat16 [4096, 6, 2048], P(('sp', 'tp'))
- log_weight: float32 [4096, 6, 8], P('sp', None, 'tp')
All inputs are finite; a program needn't handle non-finite values.
Results may differ from a plain program's by a relative error of at most 0.015.
Values may be sent and summed in bfloat16 or wider, within the bound.
A program may use at most 128 MiB of HBM per device.

v0:
```python
import math

import jax
import jax.numpy as jnp
from jax import lax
from jax.sharding import PartitionSpec as P

GROUPS = 3
HEADS = 8
STEPS = 24
DILATION_MIDDLE = 4
DILATION_WIDE = 16


epsilon = 1e-06


def from_behind(block, axis, distance):
    devices = range(lax.axis_size(axis))
    route = [(i - distance, i) for i in devices if i - distance in devices]
    return lax.ppermute(block, axis, route)


def laid_out(tiles, dim):
    shape = list(tiles.shape[1:])
    shape[dim] *= tiles.shape[0]
    return jnp.moveaxis(tiles, 0, dim).reshape(shape)


def one_gather(arrays, axis, dims):
    vector = jnp.concatenate([a.reshape(-1) for a in arrays])
    lines, at, gathered = lax.all_gather(vector, axis), 0, []
    for a, dim in zip(arrays, dims):
        tiles = lines[:, at : at + a.size].reshape(-1, *a.shape)
        gathered.append(laid_out(tiles, dim))
        at += a.size
    return tuple(gathered)


def gathered_then(shard, axis, dim, work):
    return work(lax.all_gather(shard, axis, axis=dim, tiled=True), jnp.int32(0))


def scattered(portion, width, axis):
    count = width * lax.axis_size(axis)
    sent = portion(jnp.int32(0), count).astype(jnp.bfloat16)
    return lax.psum_scatter(sent, axis, scatter_dimension=0, tiled=True).astype(jnp.float32)


def rms_normed(values, gain):
    widened = values.astype(jnp.float32)
    scaled = widened * lax.rsqrt(jnp.mean(widened * widened, axis=-1, keepdims=True) + epsilon)
    return (scaled * gain.astype(jnp.float32)).astype(jnp.bfloat16)


def reach_back(pairs, reaches):
    local_rows = pairs.shape[0]
    holding = pairs
    covered = 1
    while covered < max(reaches) + 1:
        arrived = from_behind(holding, "sp", covered)
        holding = jnp.concatenate((arrived, holding), 0)
        covered = covered * 2
    held_rows = holding.shape[0]
    extended = [
        holding[held_rows - (reach + 1) * local_rows :, :, :, group_index]
        for group_index, reach in enumerate(reaches)
    ]
    return extended


def attend_group(queries, extended, reach, dilation):
    local_rows, batch_count, local_heads, head_width = queries.shape
    span_rows = extended.shape[0]
    keys = extended[:, :, 0].reshape(
        span_rows // dilation, dilation, batch_count, local_heads, head_width
    )
    values = extended[:, :, 1].reshape(
        span_rows // dilation, dilation, batch_count, local_heads, head_width
    )
    strided = queries.reshape(
        local_rows // dilation, dilation, batch_count, local_heads, head_width
    )
    scores = jnp.einsum("qrbhe,krbhe->rbhqk", strided, keys, preferred_element_type=jnp.float32)
    scores = scores * (1.0 / math.sqrt(head_width))
    shape_steps = (local_rows // dilation, span_rows // dilation)
    query_step = lax.broadcasted_iota(jnp.int32, shape_steps, 0)
    key_step = lax.broadcasted_iota(jnp.int32, shape_steps, 1)
    lag_steps = query_step + reach * (local_rows // dilation) - key_step
    anchor = (lax.axis_index("sp") - reach) * (local_rows // dilation)
    allowed = (lag_steps >= 0) & (lag_steps <= STEPS) & (key_step + anchor >= 0)
    scores = jnp.where(allowed, scores, jnp.float32(-1e30))
    peak = jnp.max(scores, axis=-1, keepdims=True)
    lifted = jnp.exp(scores - peak)
    totals = jnp.sum(lifted, axis=-1, keepdims=True)
    log_sum = (peak + jnp.log(totals))[..., 0]
    weights = (lifted / totals).astype(jnp.bfloat16)
    mixed = jnp.einsum(
        "rbhqk,krbhe->qrbhe", weights, values, preferred_element_type=jnp.float32
    ).astype(jnp.bfloat16)
    mixed = mixed.reshape(local_rows, batch_count, local_heads, head_width)
    log_rows = jnp.transpose(log_sum, (3, 0, 1, 2)).reshape(local_rows, batch_count, local_heads)
    return (mixed, log_rows)


def shards(tokens, norm_gain, w_query, w_key, w_value, w_out):
    query_full, key_full, value_full, out_full = one_gather(
        (w_query, w_key, w_value, w_out), "sp", (1, 1, 1, 1)
    )
    roles = jnp.stack((query_full, key_full, value_full))
    normed = rms_normed(tokens, norm_gain)

    def project(piece, start):
        return jnp.einsum(
            "tbd,rgdc->tbrgc", piece, roles, preferred_element_type=jnp.float32
        ).astype(jnp.bfloat16)

    projected = gathered_then(normed, "tp", 0, project)
    local_rows = projected.shape[0]
    batch_count = projected.shape[1]
    local_heads = HEADS // lax.axis_size("tp")
    head_width = projected.shape[-1] // local_heads
    dilations = (1, DILATION_MIDDLE, DILATION_WIDE)
    reaches = tuple((-(-STEPS * dilation // local_rows) for dilation in dilations))
    pairs = projected[:, :, 1:]
    extended = [
        reach_back(pairs[:, :, :, group_index : group_index + 1], (reaches[group_index],))[0]
        for group_index in range(GROUPS)
    ]
    results = []
    for group_index in range(GROUPS):
        queries = projected[:, :, 0, group_index].reshape(
            local_rows, batch_count, local_heads, head_width
        )
        results.append(
            attend_group(
                queries, extended[group_index], reaches[group_index], dilations[group_index]
            )
        )
    stacked_logs = jnp.stack([result[1] for result in results])
    top_log = jnp.max(stacked_logs, axis=0)
    log_weight = top_log + jnp.log(jnp.sum(jnp.exp(stacked_logs - top_log[None]), axis=0))
    shares = jax.nn.softmax(stacked_logs, axis=0)
    outputs = jnp.stack([result[0] for result in results]).astype(jnp.float32)
    combined = jnp.sum(shares[..., None] * outputs, axis=0).astype(jnp.bfloat16)
    combined = combined.reshape(local_rows, batch_count, local_heads * head_width)

    def output_rows(begin, count):
        selected = lax.dynamic_slice_in_dim(combined, begin, count, 0)
        return jnp.einsum("tbc,cd->tbd", selected, out_full, preferred_element_type=jnp.float32)

    mixed = scattered(output_rows, local_rows // lax.axis_size("tp"), "tp").astype(jnp.bfloat16)
    return (mixed, log_weight)


def solution(mesh):
    in_specs = (
        P(("sp", "tp"), None, None),
        P(),
        P(None, "sp", "tp"),
        P(None, "sp", "tp"),
        P(None, "sp", "tp"),
        P("tp", "sp"),
    )
    out_specs = (P(("sp", "tp"), None, None), P("sp", None, "tp"))
    return jax.shard_map(shards, mesh=mesh, in_specs=in_specs, out_specs=out_specs, check_vma=False)
```

profile of v0, /device:TPU:1, one launch (start us, length us, event | category | flops | bytes accessed | tf_op | source)
XLA Modules:
  0.0 261.2 jit_solution(15184111302109803519)
XLA Ops:
  15.3 58.0 %all-gather.6.cloned.1.call-done = bf16[5242880]{0:T(1024)(128)(2,1)} async-done(((bf16[163840]{0:T(1024)(128)(2,1)}), bf16[5242880]{0:T(1024)(128)(2,1)}) %all-gather.6.cloned.1.call-update) | async-done | bytes 10485776 | tf_op jit(solution)/shard_map/all_gather | solution.py:32
  73.3 10.2 %reshape.177 = bf16[32,163840]{1,0:T(8,128)(2,1)} reshape(bf16[5242880]{0:T(1024)(128)(2,1)} %all-gather.6.cloned.1.call-done) | data formatting | bytes 20971520 | tf_op jit(solution)/shard_map/all_gather | solution.py:32
  83.5 4.1 %fusion.62 = (bf16[32,49152]{1,0:T(8,128)(2,1)S(1)}, bf16[32,49152]{1,0:T(8,128)(2,1)S(1)}, bf16[32,49152]{1,0:T(8,128)(2,1)S(1)}) fusion(bf16[32,163840]{1,0:T(8,128)(2,1)} %reshape.177), kind=kLoop, calls=%fused_computation.88 | loop fusion | bytes 18874368 | tf_op jit(solution)/shard_map/slice | solution.py:34
  89.4 2.2 copy.49
  92.3 2.0 copy.48
  94.3 19.4 %all-gather.4.cloned.1.call-done = bf16[128,6,2048]{2,0,1:T(8,128)(2,1)} async-done(((bf16[32,6,2048]{2,0,1:T(8,128)(2,1)}), bf16[128,6,2048]{2,0,1:T(8,128)(2,1)}) %all-gather.4.cloned.1.call-update) | async-done | bytes 3145744 | tf_op jit(solution)/shard_map/all_gather | solution.py:41
  113.7 11.4 %fusion.6 = bf16[128,6,3,3,256]{4,0,3,2,1:T(8,128)(2,1)S(1)} fusion(bf16[1,3,2048,256]{3,2,1,0:T(8,128)(2,1)} %bitcast.135, bf16[1,3,2048,256]{3,2,1,0:T(8,128)(2,1)} %bitcast.136, bf16[1,3,2048,256]{3,2,1,0:T(8,128)(2,1)S(1)} %bitcast.134, bf16[128,6,2048]{2,0,1:T(8,128)(2,1)} %all-gather.4.cloned.1.call-done), kind=kOutput, calls=%fused_computation.9 | convolution fusion | flops 7277838336 | bytes 16121856 | tf_op jit(solution)/shard_map/tbd,rgdc->tbrgc/dot_general | solution.py:114
  125.1 1.5 fusion.64
  127.7 3.9 %collective-permute-start.1 = (bf16[128,6,2,1,256]{4,0,3,2,1:T(8,128)(2,1)}, bf16[128,6,2,1,256]{4,0,3,2,1:T(8,128)(2,1)}, u32[]{:S(2)}, u32[]{:S(2)}) collective-permute-start(bf16[128,6,2,1,256]{4,0,3,2,1:T(8,128)(2,1)} %get-tuple-element.12), channel_id=1, source_target_pairs={{0,4},{4,8},{8,12},{12,16},{16,20},{20,24},{24,28},{28,32},{32,36}... | collective-permute-start | bytes 2359304 | tf_op jit(solution)/shard_map/ppermute | solution.py:21
  132.4 2.3 reshape.175
  134.7 1.6 copy.67
  136.3 1.4 fusion.63
  139.5 1.9 collective-permute-start
  141.5 3.7 %collective-permute-start.2 = (bf16[128,6,2,1,256]{4,0,3,2,1:T(8,128)(2,1)S(1)}, bf16[128,6,2,1,256]{4,0,3,2,1:T(8,128)(2,1)S(1)}, u32[]{:S(2)}, u32[]{:S(2)}) collective-permute-start(bf16[128,6,2,1,256]{4,0,3,2,1:T(8,128)(2,1)S(1)} %copy-done), channel_id=1, source_target_pairs={{0,4},{4,8},{8,12},{12,16},{16,20},{20,24},{24,28},{28,32},{32,36}... | collective-permute-start | bytes 2359304 | tf_op jit(solution)/shard_map/ppermute | solution.py:21
  145.2 1.5 maximum_bitcast_fusion.6
  147.6 2.7 %reshape_squeeze.14 = bf16[64,4,6,2,128]{4,3,1,0,2:T(2,128)(2,1)} reshape(bf16[256,6,1,256]{3,0,2,1:T(8,128)(2,1)} %get-tuple-element.17) | data formatting | bytes 1572864 | tf_op jit(solution)/shard_map/reshape;squeeze | solution.py:75
  150.3 1.8 fusion.69
  154.7 4.1 %collective-permute-done.2 = bf16[128,6,2,1,256]{4,0,3,2,1:T(8,128)(2,1)S(1)} collective-permute-done((bf16[128,6,2,1,256]{4,0,3,2,1:T(8,128)(2,1)S(1)}, bf16[128,6,2,1,256]{4,0,3,2,1:T(8,128)(2,1)S(1)}, u32[]{:S(2)}, u32[]{:S(2)}) %collective-permute-start.2) | collective-permute-done | bytes 786464 | tf_op jit(solution)/shard_map/ppermute | solution.py:21
  160.0 4.3 %collective-permute-start.3 = (bf16[256,6,2,1,256]{4,0,3,2,1:T(8,128)(2,1)}, bf16[256,6,2,1,256]{4,0,3,2,1:T(8,128)(2,1)}, u32[]{:S(2)}, u32[]{:S(2)}) collective-permute-start(bf16[256,6,2,1,256]{4,0,3,2,1:T(8,128)(2,1)} %pad_maximum_fusion), channel_id=1, source_target_pairs={{0,8},{4,12},{8,16},{12,20},{16,24},{20,28},{24,32},{28,36},{32,40... | collective-permute-start | bytes 4718600 | tf_op jit(solution)/shard_map/ppermute | solution.py:21
  166.5 2.7 %reshape.173 = bf16[256,6,2,128]{3,2,0,1:T(2,128)(2,1)} reshape(bf16[256,6,1,256]{3,0,2,1:T(8,128)(2,1)} %get-tuple-element.15) | data formatting | bytes 1572864 | tf_op jit(solution)/shard_map/reshape.1
  170.6 1.8 fusion.31
  173.0 1.6 fusion.70
  175.7 1.5 fusion.30
  177.2 18.4 %collective-permute-done.3 = bf16[256,6,2,1,256]{4,0,3,2,1:T(8,128)(2,1)} collective-permute-done((bf16[256,6,2,1,256]{4,0,3,2,1:T(8,128)(2,1)}, bf16[256,6,2,1,256]{4,0,3,2,1:T(8,128)(2,1)}, u32[]{:S(2)}, u32[]{:S(2)}) %collective-permute-start.3) | collective-permute-done | bytes 1572896 | tf_op jit(solution)/shard_map/ppermute | solution.py:21
  195.7 1.5 maximum_bitcast_fusion.2
  197.2 1.4 fusion.65
  198.5 2.4 reshape_squeeze.15
  200.9 2.1 fusion.68
  205.0 1.9 reshape_squeeze.17
  206.9 2.3 fusion.27
  211.0 2.7 %convolution_convert_fusion = bf16[128,6,2048]{2,0,1:T(8,128)(2,1)} fusion(bf16[128,6,256]{0,2,1:T(8,128)(2,1)S(1)} %bitcast.137, bf16[256,2048,1]{0,1,2:T(8,128)(2,1)S(1)} %bitcast.133), kind=kOutput, calls=%fused_computation.6 | convolution fusion | flops 806879232 | bytes 4587520 | tf_op jit(solution)/shard_map/tbc,cd->tbd/dot_general | solution.py:150
  214.3 40.4 %reduce-scatter.2.cloned.1.call-done = bf16[32,6,2048]{2,0,1:T(8,128)(2,1)} async-done(((bf16[128,6,2048]{2,0,1:T(8,128)(2,1)}), bf16[32,6,2048]{2,0,1:T(8,128)(2,1)}) %reduce-scatter.2.cloned.1.call-update) | async-done | bytes 786448 | tf_op jit(solution)/shard_map/reduce_scatter | solution.py:47
  (98 shorter events, 28.4 us)
Async XLA Ops:
  7.2 6.2 %copy-start.3 = (bf16[32,6,2048]{2,0,1:T(8,128)(2,1)S(1)}, bf16[32,6,2048]{2,0,1:T(8,128)(2,1)}, u32[]{:S(2)}) copy-start(bf16[32,6,2048]{2,0,1:T(8,128)(2,1)} %param.6) | copy-start | bytes 2359300
  7.2 6.2 %copy-start.17 = (f32[2048]{0:T(1024)S(1)}, f32[2048]{0:T(1024)}, u32[]{:S(2)}) copy-start(f32[2048]{0:T(1024)} %param.7) | copy-start | bytes 24580
  7.2 66.1 %all-gather.6.cloned.1.call-start = ((), (), s32[]{:S(2)}) async-start(), calls=%async_computation.3 | async-start | bytes 10813440 | tf_op jit(solution)/shard_map/all_gather | solution.py:32
  12.0 101.7 %all-gather.4.cloned.1.call-start = ((), (), s32[]{:S(2)}) async-start(), calls=%async_computation.1 | async-start | bytes 3932160 | tf_op jit(solution)/shard_map/all_gather | solution.py:41
  14.6 240.1 %reduce-scatter.2.cloned.1.call-start = ((), (), s32[]{:S(2)}) async-start(), calls=%async_computation.2 | async-start | bytes 3932160 | tf_op jit(solution)/shard_map/reduce_scatter | solution.py:47
  125.1 2.6 copy-start.2
  125.1 7.3 %slice-start = ((bf16[32,163840]{1,0:T(8,128)(2,1)}), bf16[32,16384]{1,0:T(8,128)(2,1)S(1)}, s32[]{:S(2)}) async-start(bf16[32,163840]{1,0:T(8,128)(2,1)} %reshape.177), calls=%async_computation.4 | async-start | bytes 2097152 | tf_op jit(solution)/shard_map/slice | solution.py:34
  127.7 17.5 %collective-permute-start.1 = (bf16[128,6,2,1,256]{4,0,3,2,1:T(8,128)(2,1)}, bf16[128,6,2,1,256]{4,0,3,2,1:T(8,128)(2,1)}, u32[]{:S(2)}, u32[]{:S(2)}) collective-permute-start(bf16[128,6,2,1,256]{4,0,3,2,1:T(8,128)(2,1)} %get-tuple-element.12), channel_id=1, source_target_pairs={{0,4},{4,8},{8,12},{12,16},{16,20},{20,24},{24,28},{28,32},{32,36}... | collective-permute-start | bytes 2359304 | tf_op jit(solution)/shard_map/ppermute | solution.py:21
  136.3 3.2 %copy-start.4 = (bf16[128,6,2,1,256]{4,0,3,2,1:T(8,128)(2,1)S(1)}, bf16[128,6,2,1,256]{4,0,3,2,1:T(8,128)(2,1)}, u32[]{:S(2)}) copy-start(bf16[128,6,2,1,256]{4,0,3,2,1:T(8,128)(2,1)} %get-tuple-element.10) | copy-start | bytes 2359300
  136.3 5.1 %copy-start = (bf16[128,6,2,1,256]{4,0,3,2,1:T(8,128)(2,1)S(1)}, bf16[128,6,2,1,256]{4,0,3,2,1:T(8,128)(2,1)}, u32[]{:S(2)}) copy-start(bf16[128,6,2,1,256]{4,0,3,2,1:T(8,128)(2,1)} %get-tuple-element.11) | copy-start | bytes 2359300
  139.5 24.8 %collective-permute-start = (bf16[128,6,2,1,256]{4,0,3,2,1:T(8,128)(2,1)S(1)}, bf16[128,6,2,1,256]{4,0,3,2,1:T(8,128)(2,1)}, u32[]{:S(2)}, u32[]{:S(2)}) collective-permute-start(bf16[128,6,2,1,256]{4,0,3,2,1:T(8,128)(2,1)S(1)} %copy-done.4), channel_id=1, source_target_pairs={{0,4},{4,8},{8,12},{12,16},{16,20},{20,24},{24,28},{28,32},{32,36}... | collective-permute-start | bytes 2359304 | tf_op jit(solution)/shard_map/ppermute | solution.py:21
  141.5 17.3 %collective-permute-start.2 = (bf16[128,6,2,1,256]{4,0,3,2,1:T(8,128)(2,1)S(1)}, bf16[128,6,2,1,256]{4,0,3,2,1:T(8,128)(2,1)S(1)}, u32[]{:S(2)}, u32[]{:S(2)}) collective-permute-start(bf16[128,6,2,1,256]{4,0,3,2,1:T(8,128)(2,1)S(1)} %copy-done), channel_id=1, source_target_pairs={{0,4},{4,8},{8,12},{12,16},{16,20},{20,24},{24,28},{28,32},{32,36}... | collective-permute-start | bytes 2359304 | tf_op jit(solution)/shard_map/ppermute | solution.py:21
  152.1 0.9 copy-start.9
  152.1 0.9 copy-start.12
  160.0 35.6 %collective-permute-start.3 = (bf16[256,6,2,1,256]{4,0,3,2,1:T(8,128)(2,1)}, bf16[256,6,2,1,256]{4,0,3,2,1:T(8,128)(2,1)}, u32[]{:S(2)}, u32[]{:S(2)}) collective-permute-start(bf16[256,6,2,1,256]{4,0,3,2,1:T(8,128)(2,1)} %pad_maximum_fusion), channel_id=1, source_target_pairs={{0,8},{4,12},{8,16},{12,20},{16,24},{20,28},{24,32},{28,36},{32,40... | collective-permute-start | bytes 4718600 | tf_op jit(solution)/shard_map/ppermute | solution.py:21
  166.5 4.1 %copy-start.13 = (f32[4,6,2,32]{3,2,1,0:T(2,128)S(1)}, f32[4,6,2,32]{3,2,1,0:T(2,128)}, u32[]{:S(2)}) copy-start(f32[4,6,2,32]{3,2,1,0:T(2,128)} %copy-done.12) | copy-start | bytes 18436
  170.6 2.4 copy-start.11
  173.0 2.7 %copy-start.10 = (bf16[256,6,1,256]{0,3,1,2:T(8,128)(2,1)S(1)}, bf16[256,6,1,256]{0,3,1,2:T(8,128)(2,1)}, u32[]{:S(2)}) copy-start(bf16[256,6,1,256]{0,3,1,2:T(8,128)(2,1)} %copy.73) | copy-start | bytes 2359300
  203.1 0.9 copy-start.5
  203.1 1.5 copy-start.7
  204.6 2.3 copy-start.6
  204.7 2.2 copy-start.8
  206.9 2.8 %copy-start.15 = (f32[128,6,2]{0,2,1:T(2,128)S(1)}, f32[128,6,2]{0,2,1:T(2,128)}, u32[]{:S(2)}) copy-start(f32[128,6,2]{0,2,1:T(2,128)} %reduce_max.61) | copy-start | bytes 18436
  206.9 2.8 %copy-start.14 = (f32[1,128,6,2]{1,3,2,0:T(2,128)S(1)}, f32[1,128,6,2]{1,3,2,0:T(2,128)}, u32[]{:S(2)}) copy-start(f32[1,128,6,2]{1,3,2,0:T(2,128)} %stack.17) | copy-start | bytes 18436
  206.9 2.8 %copy-start.16 = (f32[1,128,6,2]{1,3,2,0:T(2,128)S(1)}, f32[1,128,6,2]{1,3,2,0:T(2,128)}, u32[]{:S(2)}) copy-start(f32[1,128,6,2]{1,3,2,0:T(2,128)} %fusion.58) | copy-start | bytes 18436
  209.2 1.8 copy-start.1
Sparse Core Ops, SparseCore 0:
  12.1 61.1 all-gather.5
  75.5 38.1 all-gather.3
  213.8 40.8 reduce-scatter.1
where the time goes:
time: 262 us; the launch traced here: 261 us
  waiting for transfers between devices  140 us (53%)
  local copies, waits for them, and re-layouts  53.1 us (20%)
  matrix products  25.2 us (10%)
  other arithmetic  14.5 us (6%)
  between operations  14.2 us (5%)
  starting transfers between devices  13.9 us (5%)
    all_gather x1, waiting for transfers between devices, one_gather(): lines, at, gathered = (lax.all_gather(vector, axis), 0, [])  58 us
    reduce_scatter x1, waiting for transfers between devices, scattered(): lax.psum_scatter(sent, axis, scatter_dimension=0, tiled=True)  40.4 us
    ppermute x4, waiting for transfers between devices, from_behind(): return lax.ppermute(block, axis, route)  22.5 us
    all_gather x1, waiting for transfers between devices, gathered_then(): return work(lax.all_gather(shard, axis, axis=dim, tiled=True), jnp.int32(0))  19.4 us
    ppermute x4, starting transfers between devices, from_behind(): return lax.ppermute(block, axis, route)  13.8 us
    dot_general x1, matrix products, project(): jnp.einsum('tbd,rgdc->tbrgc', piece, roles, preferred_element_type=jnp.fl...  11.4 us
    all_gather x1, local copies, waits for them, and re-layouts, one_gather(): lines, at, gathered = (lax.all_gather(vector, axis), 0, [])  10.2 us
    unnamed x43, local copies, waits for them, and re-layouts  8.43 us
  transfers between devices with their start and end apart: 7, of which 5 were waited for; matrix products, arithmetic and copies ran while one was open for 21% of the time, Pallas kernels for 0%

commit v1 on v0

v1 whole, which is shorter than its diff:
```python
import functools
import math

import jax
import jax.numpy as jnp
from jax import lax
from jax.experimental import pallas as pl
from jax.experimental.pallas import tpu as pltpu
from jax.sharding import PartitionSpec as P

GROUPS = 3
HEADS = 8
HEAD_WIDTH = 128
STEPS = 24
DILATION_MIDDLE = 4
DILATION_WIDE = 16
WIDTH = 2048
BATCH = 6
SHARE = BATCH // 2
ROWS = 512
BACK = (128, 128, 384)
USED = (32, 96, 384)
WINDOW = (256, 256, 512)
KEYS = sum(WINDOW)
BLOCK = 128
PIECE = 64
COLUMNS = 10 * HEAD_WIDTH
ABSENT = -1e30

epsilon = 1e-06
MESH = pl.DeviceIdType.MESH


def rms_normed(values, gain):
    widened = values.astype(jnp.float32)
    scaled = widened * lax.rsqrt(jnp.mean(widened * widened, axis=-1, keepdims=True) + epsilon)
    return (scaled * gain.astype(jnp.float32)).astype(jnp.bfloat16)


def dot(a, b):
    return lax.dot_general(a, b, (((1,), (0,)), ((), ())), preferred_element_type=jnp.float32)


def dot_t(a, b):
    return lax.dot_general(a, b, (((1,), (1,)), ((), ())), preferred_element_type=jnp.float32)


def kernel(
    normed, piece, out, logs,
    toks, weights, whole_out, queries, near, middle, wide, bias, combined, arrived,
    log_rows, own_sem, send_sem, recv_sem,
):
    s, x = lax.axis_index("sp"), lax.axis_index("tp")
    core, chip = lax.rem(s, 2), lax.div(s, 2)
    y, z = lax.rem(chip, 4), lax.div(chip, 4)

    def turn(value, by):
        return lax.rem(value + (by + 4), 4)

    def spot(y_at, z_at, core_at):
        return (z_at * 4 + y_at) * 2 + core_at

    yp, ym, zp, zm, xp, xm = (turn(v, d) for v in (y, z, x) for d in (1, -1))
    line = lax.rem(y, 2)
    pair_y = y + 1 - 2 * line
    share = lax.rem(lax.div(y + 1, 2), 2)
    other = 1 - core
    partner = (spot(y, z, other), x)
    y_plus, y_minus = (spot(yp, z, core), x), (spot(ym, z, core), x)
    z_plus, z_minus = (spot(y, zp, core), x), (spot(y, zm, core), x)
    x_plus, x_minus = (s, xp), (s, xm)
    upper = lax.div(y, 2)
    later = (spot(3 - y, turn(z, upper), core), x)
    corner = (spot(3 - y, turn(z, 2 * upper - 1), core), x)
    across = (spot(turn(pair_y, 2), z, core), x)
    head = 2 * x + core

    crowd = []
    for flip_line in (0, 1):
        for flip_core in (0, 1):
            for step in range(4):
                if flip_line or flip_core or step:
                    y_at = pair_y if flip_line else y
                    core_at = other if flip_core else core
                    crowd.append((flip_line, flip_core, step, (spot(y_at, z, core_at), turn(x, step))))
    far_y = (spot(turn(y, 2 * line - 1), z, core), x)
    greeted = [c[3] for c in crowd] + [far_y, z_plus, z_minus, corner]

    barrier = pltpu.get_barrier_semaphore()
    for device in greeted:
        pl.semaphore_signal(barrier, inc=1, device_id=device, device_id_type=MESH)

    started = []

    class Transfer:
        def __init__(self):
            self.index = len(started)
            started.append(self)

        def start(self, src, dst, device):
            self.copy = pltpu.make_async_remote_copy(
                src_ref=src, dst_ref=dst, send_sem=send_sem.at[self.index],
                recv_sem=recv_sem.at[self.index], device_id=device, device_id_type=MESH,
            )
            self.copy.start()
            return self

        def arrive(self):
            self.copy.wait_recv()

    def send(src, dst, device):
        return Transfer().start(src, dst, device)

    def weight_rows(s_at, half=None):
        at, count = s_at * PIECE, PIECE
        if half is not None:
            at, count = at + half * (PIECE // 2), PIECE // 2
        return weights.at[pl.ds(pl.multiple_of(at, 32), count), :]

    def token_rows(line_at, core_at, x_at):
        at = line_at * 256 + core_at * 128 + x_at * 32
        return toks.at[:, pl.ds(pl.multiple_of(at, 32), 32), :]

    mine_w = pltpu.make_async_copy(piece.at[core], weight_rows(s), own_sem.at[0])
    mine_t = pltpu.make_async_copy(
        normed.at[pl.ds(share * SHARE, SHARE)], token_rows(line, core, x), own_sem.at[1]
    )
    mine_w.start()
    mine_t.start()

    pl.semaphore_wait(barrier, len(greeted))

    swap = send(piece.at[other], weight_rows(s), partner)
    give = send(
        normed.at[pl.ds((1 - share) * SHARE, SHARE)],
        token_rows(line, core, x),
        (spot(pair_y, z, core), x),
    )
    mine_w.wait()

    class Ring:
        def __init__(self, rows_of, plus, minus):
            self.rows_of, self.plus, self.minus = rows_of, plus, minus
            rows = rows_of(0, None)
            self.up = send(rows, rows, plus)
            self.down = send(rows, rows, minus)

        def onward_up(self):
            self.up.arrive()
            rows = self.rows_of(-1, 0)
            self.far_up = send(rows, rows, self.plus)

        def onward_down(self):
            self.down.arrive()
            rows = self.rows_of(1, 1)
            self.far_down = send(rows, rows, self.minus)

        def onward(self):
            self.onward_up()
            self.onward_down()

        def far(self):
            self.far_up.arrive()
            self.far_down.arrive()

    def y_ring(dz, core_at):
        return Ring(
            lambda step, half: weight_rows(spot(turn(y, step), turn(z, dz), core_at), half),
            y_plus, y_minus,
        )

    def z_ring(dy, core_at):
        return Ring(
            lambda step, half: weight_rows(spot(turn(y, dy), turn(z, step), core_at), half),
            z_plus, z_minus,
        )

    own_first = y_ring(0, core)
    own_second = {0: z_ring(0, core)}
    mine_t.wait()
    first = token_rows(line, core, x)
    tok_up = [send(first, first, x_plus)]
    tok_down = [send(first, first, x_minus)]
    tok_swap = [send(first, first, partner)]
    swap.arrive()
    their_first = z_ring(0, other)
    their_second = {0: y_ring(0, other)}

    near[:, :, : BACK[0] - USED[0], :] = jnp.zeros((2, SHARE, BACK[0] - USED[0], HEAD_WIDTH), jnp.bfloat16)
    middle[:, :, : BACK[1] - USED[1], :] = jnp.zeros((2, SHARE, BACK[1] - USED[1], HEAD_WIDTH), jnp.bfloat16)
    log_rows[...] = jnp.zeros_like(log_rows)
    left = 0
    for back, window, dilation in zip(BACK, WINDOW, (1, DILATION_MIDDLE, DILATION_WIDE)):
        query_at = lax.broadcasted_iota(jnp.int32, (BLOCK, window), 0)
        key_at = lax.broadcasted_iota(jnp.int32, (BLOCK, window), 1)
        lag = query_at + back - key_at
        allowed = (lag >= 0) & (lag <= STEPS * dilation) & ((lag & (dilation - 1)) == 0)
        bias[:, left : left + window] = jnp.where(allowed, jnp.float32(0), jnp.float32(ABSENT))
        left += window

    own_first.onward()
    own_second[-1] = z_ring(-1, core)
    own_second[1] = z_ring(1, core)
    own_second[0].onward()
    their_first.onward()
    their_second[-1] = y_ring(-1, other)
    their_second[1] = y_ring(1, other)
    their_second[0].onward()

    give.arrive()
    second = token_rows(1 - line, core, x)
    tok_up.append(send(second, second, x_plus))
    tok_down.append(send(second, second, x_minus))
    tok_swap.append(send(second, second, partner))
    tok_up[0].arrive()
    rows = token_rows(line, core, xm)
    tok_far_up = send(rows, rows, x_plus)
    tok_swap.append(send(rows, rows, partner))
    tok_down[0].arrive()
    rows = token_rows(line, core, xp)
    tok_swap.append(send(rows, rows, partner))

    own_first.far()
    own_second[2] = z_ring(2, core)
    their_first.far()
    their_second[2] = y_ring(2, other)
    for step in (-1, 1):
        own_second[step].onward()
        their_second[step].onward()

    tok_down[1].arrive()
    rows = token_rows(1 - line, core, xp)
    tok_far_down = send(rows, rows, x_minus)
    tok_swap.append(send(rows, rows, partner))
    tok_up[1].arrive()
    rows = token_rows(1 - line, core, xm)
    tok_swap.append(send(rows, rows, partner))

    own_second[2].onward()
    their_second[2].onward()
    for step in (0, -1, 1, 2):
        own_second[step].far()
        their_second[step].far()
    tok_far_up.arrive()
    rows = token_rows(line, core, turn(x, 2))
    tok_swap.append(send(rows, rows, partner))
    tok_far_down.arrive()
    rows = token_rows(1 - line, core, turn(x, 2))
    tok_swap.append(send(rows, rows, partner))

    def head_columns(x_at, core_at, half=None):
        lanes = pl.ds(pl.multiple_of((2 * x_at + core_at) * HEAD_WIDTH, HEAD_WIDTH), HEAD_WIDTH)
        if half is None:
            return whole_out.at[:, lanes]
        return whole_out.at[pl.ds(half * (WIDTH // 2), WIDTH // 2), lanes]

    out_rows = weights.at[:, 9 * HEAD_WIDTH :]
    mine_o = head_columns(x, core)
    out_up = send(out_rows, mine_o, x_plus)
    out_down = send(out_rows, mine_o, x_minus)
    out_swap = [send(out_rows, mine_o, partner)]
    whole_out[:, pl.ds(pl.multiple_of(head * HEAD_WIDTH, HEAD_WIDTH), HEAD_WIDTH)] = weights[:, 9 * HEAD_WIDTH :]

    for copy in tok_swap:
        copy.arrive()

    def project(left, width, b):
        return dot(toks[b], weights[:, left : left + width]).astype(jnp.bfloat16)

    halo = []
    for place, keys in enumerate((wide, middle, near)):
        back, used = BACK[2 - place], USED[2 - place]

        def fill(b, carry, keys=keys, back=back, place=place):
            both = project(place * 2 * HEAD_WIDTH, 2 * HEAD_WIDTH, b)
            keys[0, b, back:, :] = both[:, :HEAD_WIDTH]
            keys[1, b, back:, :] = both[:, HEAD_WIDTH:]
            return carry

        lax.fori_loop(0, SHARE, fill, 0)
        halo.append(
            send(
                keys.at[:, :, back + ROWS - used :, :],
                keys.at[:, :, back - used : back, :],
                later,
            )
        )

    def ask(b, carry):
        both = project(6 * HEAD_WIDTH, 2 * HEAD_WIDTH, b)
        queries[2, b] = both[:, :HEAD_WIDTH]
        queries[1, b] = both[:, HEAD_WIDTH:]
        queries[0, b] = project(8 * HEAD_WIDTH, HEAD_WIDTH, b)
        return carry

    lax.fori_loop(0, SHARE, ask, 0)

    out_up.arrive()
    rows = head_columns(xm, core, 0)
    out_far_up = send(rows, rows, x_plus)
    rows = head_columns(xm, core)
    out_swap.append(send(rows, rows, partner))
    out_down.arrive()
    rows = head_columns(xp, core, 1)
    out_far_down = send(rows, rows, x_minus)
    rows = head_columns(xp, core)
    out_swap.append(send(rows, rows, partner))

    for copy in halo:
        copy.arrive()

    factor = math.log2(math.e) / math.sqrt(HEAD_WIDTH)
    start_at = (z * 2 + upper) * ROWS

    def attend(index, carry):
        b, block = lax.div(index, 4), lax.rem(index, 4)
        at = pl.multiple_of(block * BLOCK, BLOCK)
        scores, left = [], 0
        for group, keys in enumerate((near, middle, wide)):
            window = WINDOW[group]
            score = dot_t(queries[group, b, pl.ds(at, BLOCK), :], keys[0, b, pl.ds(at, window), :])
            key_at = lax.broadcasted_iota(jnp.int32, (1, window), 1) + (start_at + at - BACK[group])
            edge = jnp.where(key_at >= 0, jnp.float32(0), jnp.float32(ABSENT))
            scores.append(score * factor + (bias[:, left : left + window] + edge))
            left += window
        peak = functools.reduce(
            jnp.maximum, [jnp.max(score, axis=1, keepdims=True) for score in scores]
        )
        total, mixed = 0.0, 0.0
        for group, keys in enumerate((near, middle, wide)):
            lifted = jnp.exp2(scores[group] - peak)
            total = total + jnp.sum(lifted, axis=1, keepdims=True)
            mixed = mixed + dot(lifted.astype(jnp.bfloat16), keys[1, b, pl.ds(at, WINDOW[group]), :])
        combined[b, pl.ds(at, BLOCK), :] = (mixed / total).astype(jnp.bfloat16)
        log = (peak + jnp.log2(total)) * math.log(2.0)
        log_rows[block, pl.ds(b, 1), :] = jnp.transpose(
            jnp.broadcast_to(log, (BLOCK, BLOCK))
        )[0:1, :]
        return carry

    lax.fori_loop(0, SHARE * 4, attend, 0)

    lanes = pl.ds(pl.multiple_of(head * HEAD_WIDTH, HEAD_WIDTH), HEAD_WIDTH)
    mine = arrived.at[pl.ds(share * SHARE, SHARE), :, lanes]

    def rows_for(line_at, core_at, x_at):
        return pl.ds(pl.multiple_of(line_at * 256 + core_at * 128 + x_at * 32, 32), 32)

    exchange = []
    for flip_line, flip_core, step, device in crowd:
        line_at = 1 - line if flip_line else line
        core_at = other if flip_core else core
        exchange.append(
            send(combined.at[:, rows_for(line_at, core_at, turn(x, step)), :], mine, device)
        )
        if step == 0:
            exchange.append(send(log_rows.at[line_at * 2 + core_at], logs.at[core, share], device))
    arrived[pl.ds(share * SHARE, SHARE), :, lanes] = combined[:, rows_for(line, core, x), :]
    logs[core, share] = log_rows[line * 2 + core]

    out_far_up.arrive()
    rows = head_columns(turn(x, 2), core, 0)
    out_swap.append(send(rows, rows, partner))
    out_far_down.arrive()
    rows = head_columns(turn(x, 2), core, 1)
    out_swap.append(send(rows, rows, partner))
    for copy in out_swap + exchange:
        copy.arrive()

    to_row = lax.broadcasted_iota(jnp.int32, (256, 192), 0)
    from_row = lax.broadcasted_iota(jnp.int32, (256, 192), 1)
    chosen = ((from_row & 31) == (to_row >> 3)) & ((from_row >> 5) == (to_row & 7))
    order = jnp.where(chosen, jnp.float32(1), jnp.float32(0)).astype(jnp.bfloat16)
    ordered = dot(order, arrived[...].reshape(192, HEADS * HEAD_WIDTH)).astype(jnp.bfloat16)
    for tile in range(8):
        part = dot_t(ordered, whole_out[tile * 256 : (tile + 1) * 256, :])
        part = part.reshape(32, 8, 256)[:, :BATCH, :]
        out[:, :, tile * 256 : (tile + 1) * 256] = part.astype(jnp.bfloat16)

    for transfer in started:
        transfer.copy.wait_send()


TRANSFERS = 100


def shards(tokens, norm_gain, w_query, w_key, w_value, w_out):
    normed = jnp.transpose(rms_normed(tokens, norm_gain), (1, 0, 2))
    turned = jnp.transpose(w_out)
    halves = []
    for core in range(2):
        lanes = slice(core * HEAD_WIDTH, (core + 1) * HEAD_WIDTH)
        parts = []
        for group in (2, 1, 0):
            parts += [w_key[group, :, lanes], w_value[group, :, lanes]]
        parts += [w_query[group, :, lanes] for group in (2, 1, 0)]
        halves.append(jnp.concatenate(parts + [turned[:, lanes]], axis=1))
    piece = jnp.stack(halves)

    bf16, f32 = jnp.bfloat16, jnp.float32
    mixed, logs = pl.pallas_call(
        kernel,
        out_shape=(
            jax.ShapeDtypeStruct((32, BATCH, WIDTH), bf16),
            jax.ShapeDtypeStruct((2, 2, 8, 128), f32),
        ),
        in_specs=[pl.BlockSpec(memory_space=pl.ANY)] * 2,
        out_specs=[pl.BlockSpec(memory_space=pltpu.VMEM)] * 2,
        scratch_shapes=[
            pltpu.VMEM((SHARE, ROWS, WIDTH), bf16),
            pltpu.VMEM((WIDTH, COLUMNS), bf16),
            pltpu.VMEM((WIDTH, HEADS * HEAD_WIDTH), bf16),
            pltpu.VMEM((GROUPS, SHARE, ROWS, HEAD_WIDTH), bf16),
            pltpu.VMEM((2, SHARE, BACK[0] + ROWS, HEAD_WIDTH), bf16),
            pltpu.VMEM((2, SHARE, BACK[1] + ROWS, HEAD_WIDTH), bf16),
            pltpu.VMEM((2, SHARE, BACK[2] + ROWS, HEAD_WIDTH), bf16),
            pltpu.VMEM((BLOCK, KEYS), f32),
            pltpu.VMEM((SHARE, ROWS, HEAD_WIDTH), bf16),
            pltpu.VMEM((BATCH, 32, HEADS * HEAD_WIDTH), bf16),
            pltpu.VMEM((4, 8, 128), f32),
            pltpu.SemaphoreType.DMA((2,)),
            pltpu.SemaphoreType.DMA((TRANSFERS,)),
            pltpu.SemaphoreType.DMA((TRANSFERS,)),
        ],
        compiler_params=pltpu.CompilerParams(
            collective_id=0, has_side_effects=True, vmem_limit_bytes=60 * 1024 * 1024
        ),
    )(normed, piece)
    logs = logs[:, :, :SHARE, :].reshape(2, BATCH, 128)
    return (mixed, jnp.transpose(logs, (2, 1, 0)))


def solution(mesh):
    in_specs = (
        P(("sp", "tp"), None, None),
        P(),
        P(None, "sp", "tp"),
        P(None, "sp", "tp"),
        P(None, "sp", "tp"),
        P("tp", "sp"),
    )
    out_specs = (P(("sp", "tp"), None, None), P("sp", None, "tp"))
    return jax.shard_map(shards, mesh=mesh, in_specs=in_specs, out_specs=out_specs, check_vma=False)
```

time: 262 us -> 100 us (0.38)
  waiting for transfers between devices: 140 us -> 0 us
  Pallas kernels: 0 us -> 84.4 us
  local copies, waits for them, and re-layouts: 53.1 us -> 10.5 us
  matrix products: 25.2 us -> 0 us
  starting transfers between devices: 13.9 us -> 0 us
  between operations: 14.2 us -> 0.72 us
  other arithmetic: 14.5 us -> 3.36 us
    pallas_call x0 -> x1, Pallas kernels: none -> 84.4 us  [shards(): pl.pallas_call(kernel, out_shape=(jax.ShapeDtypeStruct((32, BATCH, WIDTH)...]
    all_gather x2 -> x0, waiting for transfers between devices: 77.3 us -> none  [the longest x1 58 us: one_gather(): lines, at, gathered = (lax.all_gather(vector, axis), 0, [])]
    reduce_scatter x1 -> x0, waiting for transfers between devices: 40.4 us -> none  [scattered(): lax.psum_scatter(sent, axis, scatter_dimension=0, tiled=True)]
    dot_general x8 -> x0, matrix products: 25.2 us -> none  [the longest x1 11.4 us: project(): jnp.einsum('tbd,rgdc->tbrgc', piece, roles, preferred_element_type=jnp.fl...]
    ppermute x4 -> x0, waiting for transfers between devices: 22.5 us -> none  [from_behind(): return lax.ppermute(block, axis, route)]
    ppermute x4 -> x0, starting transfers between devices: 13.8 us -> none  [from_behind(): return lax.ppermute(block, axis, route)]
    another operation x12 -> x0, local copies, waits for them, and re-layouts: 13.2 us -> none  [the longest x2 5.06 us: attend_group(): extended[:, :, 0]]
    all_gather x1 -> x0, local copies, waits for them, and re-layouts: 10.2 us -> none  [one_gather(): lines, at, gathered = (lax.all_gather(vector, axis), 0, [])]
  transfers between devices with their start and end apart: 7 -> 0, of which waited for: 5 -> 0; matrix products, arithmetic and copies ran while one was open for 21% -> 0% of each run, Pallas kernels for 0% -> 0%
where the time goes in v1:
time: 100 us; the launch traced here: 99 us
  Pallas kernels  84.4 us (84%)
  local copies, waits for them, and re-layouts  10.5 us (10%)
  other arithmetic  3.36 us (3%)
    pallas_call x1, Pallas kernels, shards(): pl.pallas_call(kernel, out_shape=(jax.ShapeDtypeStruct((32, BATCH, WIDTH)...  84.4 us
    unnamed x25, local copies, waits for them, and re-layouts  9.92 us

profile of v1, /device:TPU:1, one launch (start us, length us, event | category | flops | bytes accessed | tf_op | source)
XLA Modules:
  0.0 99.0 jit_solution(7536334414415684420)
XLA Ops:
  0.6 0.0 copy-start.1
  0.6 0.0 copy-start.2
  0.7 0.0 copy-start
  0.7 0.0 copy-start.3
  0.7 1.4 %fusion = f32[32,6]{0,1:T(8,128)S(1)} fusion(bf16[32,6,2048]{2,0,1:T(8,128)(2,1)} %param.6), kind=kLoop, calls=%fused_computation.2 | loop fusion | flops 1179456 | bytes 787200 | tf_op jit(solution)/shard_map/reduce_sum | solution.py:36
  2.1 0.7 constant_dynamic-update-slice_fusion.9
  2.8 0.7 constant_dynamic-update-slice_fusion.8
  3.6 0.7 constant_dynamic-update-slice_fusion.7
  4.3 0.7 constant_dynamic-update-slice_fusion.6
  5.0 0.7 constant_dynamic-update-slice_fusion.5
  5.8 0.7 constant_dynamic-update-slice_fusion.4
  6.5 0.0 copy-done.1
  6.5 0.7 constant_dynamic-update-slice_fusion.3
  7.3 0.7 constant_dynamic-update-slice_fusion.16
  8.0 0.7 constant_dynamic-update-slice_fusion.15
  8.7 0.7 constant_dynamic-update-slice_fusion.14
  9.5 0.0 copy-done.2
  9.5 0.8 pad_maximum_fusion.piece
  10.3 0.0 copy-done
  10.3 0.0 copy-done.3
  10.3 1.1 %fusion.3.normed = bf16[6,32,2048]{2,1,0:T(8,128)(2,1)} fusion(bf16[32,6,2048]{2,0,1:T(8,128)(2,1)S(1)} %copy-done, f32[2048]{0:T(1024)S(1)} %copy-done.3, f32[32,6]{0,1:T(8,128)S(1)} %add_rsqrt_fusion), kind=kLoop, calls=%fused_computation.5 | loop fusion | flops 1572864 | bytes 1581824 | tf_op jit(solution)/shard_map/transpose | solution.py:388
  11.4 84.4 %shard_map.77 = (bf16[32,6,2048]{2,1,0:T(8,128)(2,1)}, f32[2,2,8,128]{3,2,1,0:T(8,128)}) custom-call(bf16[6,32,2048]{2,1,0:T(8,128)(2,1)} %fusion.3.normed, bf16[2,64,1280]{2,1,0:T(8,128)(2,1)} %pad_maximum_fusion.piece), custom_call_target="tpu_custom_call" | custom-call | tf_op jit(solution)/shard_map/pallas_call | solution.py:401
  95.9 0.0 copy-start.4
  95.9 2.5 %copy.11 = bf16[32,6,2048]{2,0,1:T(8,128)(2,1)} copy(bf16[32,6,2048]{2,1,0:T(8,128)(2,1)} %get-tuple-element.8) | data formatting | bytes 1572864
  98.4 0.0 copy-done.4
  98.4 0.6 copy.10
  (7 shorter events, 0.1 us)
Async XLA Ops:
  0.6 5.9 %copy-start.1 = (bf16[3,64,256]{2,1,0:T(8,128)(2,1)S(1)}, bf16[3,64,256]{2,1,0:T(8,128)(2,1)}, u32[]{:S(2)}) copy-start(bf16[3,64,256]{2,1,0:T(8,128)(2,1)} %param.8) | copy-start | bytes 294916
  0.6 8.9 %copy-start.2 = (bf16[256,64]{0,1:T(8,128)(2,1)S(1)}, bf16[256,64]{0,1:T(8,128)(2,1)}, u32[]{:S(2)}) copy-start(bf16[256,64]{0,1:T(8,128)(2,1)} %param.11) | copy-start | bytes 98308
  0.7 9.7 %copy-start = (bf16[32,6,2048]{2,0,1:T(8,128)(2,1)S(1)}, bf16[32,6,2048]{2,0,1:T(8,128)(2,1)}, u32[]{:S(2)}) copy-start(bf16[32,6,2048]{2,0,1:T(8,128)(2,1)} %param.6) | copy-start | bytes 2359300
  0.7 9.7 %copy-start.3 = (f32[2048]{0:T(1024)S(1)}, f32[2048]{0:T(1024)}, u32[]{:S(2)}) copy-start(f32[2048]{0:T(1024)} %param.7) | copy-start | bytes 24580
  95.9 2.6 %copy-start.4 = (f32[2,2,8,128]{3,2,1,0:T(8,128)S(1)}, f32[2,2,8,128]{3,2,1,0:T(8,128)}, u32[]{:S(2)}) copy-start(f32[2,2,8,128]{3,2,1,0:T(8,128)} %get-tuple-element.5) | copy-start | bytes 49156

commit v2 on v1

v2 whole, which is shorter than its diff:
```python
import functools
import math

import jax
import jax.numpy as jnp
from jax import lax
from jax.experimental import pallas as pl
from jax.experimental.pallas import tpu as pltpu
from jax.sharding import PartitionSpec as P

GROUPS = 3
HEADS = 8
HEAD_WIDTH = 128
STEPS = 24
DILATION_MIDDLE = 4
DILATION_WIDE = 16
WIDTH = 2048
BATCH = 6
SHARE = BATCH // 2
ROWS = 512
BACK = (128, 128, 384)
USED = (32, 96, 384)
WINDOW = (256, 256, 512)
KEYS = sum(WINDOW)
BLOCK = 128
PIECE = 64
COLUMNS = 10 * HEAD_WIDTH
ABSENT = -1e30

epsilon = 1e-06
MESH = pl.DeviceIdType.MESH


def rms_normed(widened, gain):
    scaled = widened * lax.rsqrt(jnp.mean(widened * widened, axis=-1, keepdims=True) + epsilon)
    return (scaled * gain).astype(jnp.bfloat16)


def dot(a, b):
    return lax.dot_general(a, b, (((1,), (0,)), ((), ())), preferred_element_type=jnp.float32)


def dot_t(a, b):
    return lax.dot_general(a, b, (((1,), (1,)), ((), ())), preferred_element_type=jnp.float32)


def kernel(
    tokens, gain, w_query, w_key, w_value, w_out, out, logs,
    gift, gift_out, toks, weights, whole_out, queries, near, middle, wide, bias,
    combined, arrived, log_rows, both_logs, own_sem, send_sem, recv_sem,
):
    s, x = lax.axis_index("sp"), lax.axis_index("tp")
    core, chip = lax.rem(s, 2), lax.div(s, 2)
    y, z = lax.rem(chip, 4), lax.div(chip, 4)

    def turn(value, by):
        return lax.rem(value + (by + 4), 4)

    def spot(y_at, z_at, core_at):
        return (z_at * 4 + y_at) * 2 + core_at

    zp, zm, xp, xm = (turn(v, d) for v in (z, x) for d in (1, -1))
    line = lax.rem(y, 2)
    pair_y, apart_y = y + 1 - 2 * line, turn(y, 2 * line - 1)
    share = lax.rem(lax.div(y + 1, 2), 2)
    other = 1 - core
    partner = (spot(y, z, other), x)
    z_plus, z_minus = (spot(y, zp, core), x), (spot(y, zm, core), x)
    x_plus, x_minus = (s, xp), (s, xm)
    upper = lax.div(y, 2)
    later = (spot(3 - y, turn(z, upper), core), x)
    corner = (spot(3 - y, turn(z, 2 * upper - 1), core), x)
    head = 2 * x + core

    crowd = []
    for flip_line in (0, 1):
        for flip_core in (0, 1):
            for step in range(4):
                if flip_line or flip_core or step:
                    y_at = pair_y if flip_line else y
                    core_at = other if flip_core else core
                    crowd.append((flip_line, flip_core, step, (spot(y_at, z, core_at), turn(x, step))))
    y_pair, y_apart = (spot(pair_y, z, core), x), (spot(apart_y, z, core), x)
    greeted = [c[3] for c in crowd] + [y_apart, z_plus, z_minus, corner]

    barrier = pltpu.get_barrier_semaphore()
    for device in greeted:
        pl.semaphore_signal(barrier, inc=1, device_id=device, device_id_type=MESH)

    started = []

    class Transfer:
        def __init__(self):
            self.index = len(started)
            started.append(self)

        def cover(self, src, dst, device):
            self.copy = pltpu.make_async_remote_copy(
                src_ref=src, dst_ref=dst, send_sem=send_sem.at[self.index],
                recv_sem=recv_sem.at[self.index], device_id=device, device_id_type=MESH,
            )

        def begin(self, src, dst, device):
            self.cover(src, dst, device)
            self.copy.start()

        def arrive(self):
            self.done = True
            self.copy.wait_recv()

    def send(src, dst, device):
        transfer = Transfer()
        transfer.begin(src, dst, device)
        return transfer

    def weight_rows(s_at, first=0, count=PIECE):
        return weights.at[pl.ds(pl.multiple_of(s_at * PIECE + first, 16), count), :]

    def token_rows(line_at, core_at, x_at):
        at = line_at * 256 + core_at * 128 + x_at * 32
        return toks.at[:, pl.ds(pl.multiple_of(at, 32), 32), :]

    parts = [(w, group) for group in (2, 1, 0) for w in (w_key, w_value)]
    parts += [(w_query, group) for group in (2, 1, 0)]
    rows = pl.ds(pl.multiple_of(s * PIECE, PIECE), PIECE)

    def part_of(index, core_at):
        w, group = parts[index]
        lanes = pl.ds(pl.multiple_of(core_at * HEAD_WIDTH, HEAD_WIDTH), HEAD_WIDTH)
        return (
            w.at[group, :, lanes],
            weights.at[rows, index * HEAD_WIDTH : (index + 1) * HEAD_WIDTH],
        )

    for index in range(9):
        pltpu.make_async_copy(*part_of(index, core), own_sem.at[0]).start()

    def turned(core_at):
        return w_out[:, pl.ds(pl.multiple_of(core_at * HEAD_WIDTH, HEAD_WIDTH), HEAD_WIDTH)]

    weights[rows, 9 * HEAD_WIDTH :] = turned(core)
    gift_out[...] = turned(other)
    def normed(b):
        return rms_normed(tokens[b].astype(jnp.float32), gain[...])

    place = pl.ds(pl.multiple_of(line * 256 + core * 128 + x * 32, 32), 32)
    for i in range(SHARE):
        toks[i, place, :] = normed(share * SHARE + i)
    for i in range(SHARE):
        gift[i] = normed((1 - share) * SHARE + i)

    pl.semaphore_wait(barrier, len(greeted))

    swap = Transfer()
    for index in range(9):
        src, dst = part_of(index, other)
        swap.begin(src, dst, partner)
    swap.begin(gift_out, weights.at[rows, 9 * HEAD_WIDTH :], partner)
    swap.cover(weight_rows(s), weight_rows(s), partner)
    whole = weights.at[rows, : 9 * HEAD_WIDTH]
    pltpu.make_async_copy(whole, whole, own_sem.at[0]).wait()

    class Ring:
        def __init__(self, rows_of, first, second, cut):
            self.rows_of, self.first, self.second, self.cut = rows_of, first, second, cut
            rows = rows_of(0)
            self.to_second = send(rows, rows, second)
            self.to_first = send(rows, rows, first)

        def onward(self):
            self.from_first_arrive()
            self.from_second_arrive()

    class ZRing(Ring):
        def from_first_arrive(self):
            self.to_second.arrive()
            rows = self.rows_of(-1, self.cut, PIECE - self.cut)
            self.on_second = send(rows, rows, self.second)

        def from_second_arrive(self):
            self.to_first.arrive()
            rows = self.rows_of(1, 0, self.cut)
            self.on_first = send(rows, rows, self.first)

        def far(self):
            self.on_second.arrive()
            self.on_first.arrive()

    class YRing(ZRing):
        def from_first_arrive(self):
            self.to_first.arrive()
            rows = self.rows_of("pair", self.cut, PIECE - self.cut)
            self.on_second = send(rows, rows, self.second)

        def from_second_arrive(self):
            self.to_second.arrive()
            rows = self.rows_of("apart", 0, self.cut)
            self.on_first = send(rows, rows, self.first)

    ys = {0: y, "pair": pair_y, "apart": apart_y, "far": turn(y, 2)}

    def y_ring(dz, core_at):
        return YRing(
            lambda step, *cut: weight_rows(spot(ys[step], turn(z, dz), core_at), *cut),
            y_pair, y_apart, 16,
        )

    def z_ring(dy, core_at):
        return ZRing(
            lambda step, *cut: weight_rows(spot(ys[dy], turn(z, step), core_at), *cut),
            z_minus, z_plus, 32,
        )

    own_first = y_ring(0, core)
    give = send(gift, toks.at[:, place, :], y_pair)
    own_second = {0: z_ring(0, core)}
    first = token_rows(line, core, x)
    tok_up = [send(first, first, x_plus)]
    tok_down = [send(first, first, x_minus)]
    tok_swap = [send(first, first, partner)]
    swap.arrive()
    their_first = z_ring(0, other)
    their_second = {0: y_ring(0, other)}

    near[:, :, : BACK[0] - USED[0], :] = jnp.zeros((2, SHARE, BACK[0] - USED[0], HEAD_WIDTH), jnp.bfloat16)
    middle[:, :, : BACK[1] - USED[1], :] = jnp.zeros((2, SHARE, BACK[1] - USED[1], HEAD_WIDTH), jnp.bfloat16)
    log_rows[...] = jnp.zeros_like(log_rows)
    left = 0
    for back, window, dilation in zip(BACK, WINDOW, (1, DILATION_MIDDLE, DILATION_WIDE)):
        query_at = lax.broadcasted_iota(jnp.int32, (BLOCK, window), 0)
        key_at = lax.broadcasted_iota(jnp.int32, (BLOCK, window), 1)
        lag = query_at + back - key_at
        allowed = (lag >= 0) & (lag <= STEPS * dilation) & ((lag & (dilation - 1)) == 0)
        bias[:, left : left + window] = jnp.where(allowed, jnp.float32(0), jnp.float32(ABSENT))
        left += window

    own_first.onward()
    own_second["pair"] = z_ring("pair", core)
    own_second["apart"] = z_ring("apart", core)
    own_second[0].onward()
    their_first.onward()
    their_second[-1] = y_ring(-1, other)
    their_second[1] = y_ring(1, other)
    their_second[0].onward()

    give.arrive()
    second = token_rows(1 - line, core, x)
    tok_up.append(send(second, second, x_plus))
    tok_down.append(send(second, second, x_minus))
    tok_swap.append(send(second, second, partner))
    tok_up[0].arrive()
    rows = token_rows(line, core, xm)
    tok_far_up = send(rows, rows, x_plus)
    tok_swap.append(send(rows, rows, partner))
    tok_down[0].arrive()
    rows = token_rows(line, core, xp)
    tok_swap.append(send(rows, rows, partner))

    own_first.far()
    own_second["far"] = z_ring("far", core)
    their_first.far()
    their_second[2] = y_ring(2, other)
    for y_step, z_step in (("pair", -1), ("apart", 1)):
        own_second[y_step].onward()
        their_second[z_step].onward()

    tok_down[1].arrive()
    rows = token_rows(1 - line, core, xp)
    tok_far_down = send(rows, rows, x_minus)
    tok_swap.append(send(rows, rows, partner))
    tok_up[1].arrive()
    rows = token_rows(1 - line, core, xm)
    tok_swap.append(send(rows, rows, partner))

    own_second["far"].onward()
    their_second[2].onward()
    for y_step, z_step in zip(ys, (0, -1, 1, 2)):
        own_second[y_step].far()
        their_second[z_step].far()
    tok_far_up.arrive()
    rows = token_rows(line, core, turn(x, 2))
    tok_swap.append(send(rows, rows, partner))
    tok_far_down.arrive()
    rows = token_rows(1 - line, core, turn(x, 2))
    tok_swap.append(send(rows, rows, partner))

    def head_columns(x_at, core_at, half=None):
        lanes = pl.ds(pl.multiple_of((2 * x_at + core_at) * HEAD_WIDTH, HEAD_WIDTH), HEAD_WIDTH)
        if half is None:
            return whole_out.at[:, lanes]
        return whole_out.at[pl.ds(half * (WIDTH // 2), WIDTH // 2), lanes]

    out_rows = weights.at[:, 9 * HEAD_WIDTH :]
    mine_o = head_columns(x, core)
    out_up = send(out_rows, mine_o, x_plus)
    out_down = send(out_rows, mine_o, x_minus)
    out_swap = [send(out_rows, mine_o, partner)]
    whole_out[:, pl.ds(pl.multiple_of(head * HEAD_WIDTH, HEAD_WIDTH), HEAD_WIDTH)] = weights[:, 9 * HEAD_WIDTH :]

    for copy in tok_swap:
        copy.arrive()

    def project(left, width, b):
        return dot(toks[b], weights[:, left : left + width]).astype(jnp.bfloat16)

    groups = ((wide, 2), (middle, 1), (near, 0))
    halo = []
    for b in range(SHARE):
        sent = []
        for at, (keys, group) in enumerate(groups):
            back, used = BACK[group], USED[group]
            both = project(at * 2 * HEAD_WIDTH, 2 * HEAD_WIDTH, b)
            keys[0, b, back:, :] = both[:, :HEAD_WIDTH]
            keys[1, b, back:, :] = both[:, HEAD_WIDTH:]
            sent.append(
                send(
                    keys.at[:, b, back + ROWS - used :, :],
                    keys.at[:, b, back - used : back, :],
                    later,
                )
            )
        halo.append(sent)

    def ask(b):
        both = project(6 * HEAD_WIDTH, 2 * HEAD_WIDTH, b)
        queries[2, b] = both[:, :HEAD_WIDTH]
        queries[1, b] = both[:, HEAD_WIDTH:]
        queries[0, b] = project(8 * HEAD_WIDTH, HEAD_WIDTH, b)

    ask(0)
    out_up.arrive()
    rows = head_columns(xm, core, 0)
    out_far_up = send(rows, rows, x_plus)
    rows = head_columns(xm, core)
    out_swap.append(send(rows, rows, partner))
    out_down.arrive()
    rows = head_columns(xp, core, 1)
    out_far_down = send(rows, rows, x_minus)
    rows = head_columns(xp, core)
    out_swap.append(send(rows, rows, partner))
    ask(1)
    ask(2)

    factor = math.log2(math.e) / math.sqrt(HEAD_WIDTH)
    start_at = (z * 2 + upper) * ROWS
    lanes = pl.ds(pl.multiple_of(head * HEAD_WIDTH, HEAD_WIDTH), HEAD_WIDTH)

    def rows_for(line_at, core_at, x_at):
        return pl.ds(pl.multiple_of(line_at * 256 + core_at * 128 + x_at * 32, 32), 32)

    exchange = []
    for b in range(SHARE):
        for copy in halo[b]:
            copy.arrive()

        def attend(block, carry, b=b):
            at = pl.multiple_of(block * BLOCK, BLOCK)
            scores, left = [], 0
            for group, keys in enumerate((near, middle, wide)):
                window = WINDOW[group]
                score = dot_t(queries[group, b, pl.ds(at, BLOCK), :], keys[0, b, pl.ds(at, window), :])
                key_at = lax.broadcasted_iota(jnp.int32, (1, window), 1) + (start_at + at - BACK[group])
                edge = jnp.where(key_at >= 0, jnp.float32(0), jnp.float32(ABSENT))
                scores.append(score * factor + (bias[:, left : left + window] + edge))
                left += window
            peak = functools.reduce(
                jnp.maximum, [jnp.max(score, axis=1, keepdims=True) for score in scores]
            )
            total, mixed = 0.0, 0.0
            for group, keys in enumerate((near, middle, wide)):
                lifted = jnp.exp2(scores[group] - peak)
                total = total + jnp.sum(lifted, axis=1, keepdims=True)
                mixed = mixed + dot(
                    lifted.astype(jnp.bfloat16), keys[1, b, pl.ds(at, WINDOW[group]), :]
                )
            combined[b, pl.ds(at, BLOCK), :] = (mixed / total).astype(jnp.bfloat16)
            log = (peak + jnp.log2(total)) * math.log(2.0)
            log_rows[block, b : b + 1, :] = jnp.transpose(
                jnp.broadcast_to(log, (BLOCK, BLOCK))
            )[0:1, :]
            return carry

        lax.fori_loop(0, 4, attend, 0)

        for flip_line, flip_core, step, device in crowd:
            line_at = 1 - line if flip_line else line
            core_at = other if flip_core else core
            exchange.append(
                send(
                    combined.at[b, rows_for(line_at, core_at, turn(x, step)), :],
                    arrived.at[share * SHARE + b, :, lanes],
                    device,
                )
            )
            if step == 0 and b == SHARE - 1:
                exchange.append(send(log_rows.at[line_at * 2 + core_at], both_logs.at[core, share], device))
        arrived[share * SHARE + b, :, lanes] = combined[b, rows_for(line, core, x), :]
        if b == 0:
            out_far_up.arrive()
            rows = head_columns(turn(x, 2), core, 0)
            out_swap.append(send(rows, rows, partner))
            out_far_down.arrive()
            rows = head_columns(turn(x, 2), core, 1)
            out_swap.append(send(rows, rows, partner))
    both_logs[core, share] = log_rows[line * 2 + core]
    for copy in out_swap + exchange:
        copy.arrive()

    everything = arrived[...].reshape(192, HEADS * HEAD_WIDTH)
    for tile in range(8):
        part = dot_t(everything, whole_out[tile * 256 : (tile + 1) * 256, :]).astype(jnp.bfloat16)
        out[:, :, tile * 256 : (tile + 1) * 256] = part.reshape(BATCH, 32, 256)
    for core_at in range(2):
        for share_at in range(2):
            for b in range(SHARE):
                logs[share_at * SHARE + b, core_at : core_at + 1, :] = both_logs[core_at, share_at, b : b + 1, :]

    for transfer in started:
        transfer.copy.wait_send()


TRANSFERS = 130


def shards(tokens, norm_gain, w_query, w_key, w_value, w_out):
    bf16, f32 = jnp.bfloat16, jnp.float32
    mixed, logs = pl.pallas_call(
        kernel,
        out_shape=(
            jax.ShapeDtypeStruct((BATCH, 32, WIDTH), bf16),
            jax.ShapeDtypeStruct((BATCH, 2, 128), f32),
        ),
        in_specs=[pl.BlockSpec(memory_space=pltpu.VMEM)] * 2
        + [pl.BlockSpec(memory_space=pl.ANY)] * 3
        + [pl.BlockSpec(memory_space=pltpu.VMEM)],
        out_specs=[pl.BlockSpec(memory_space=pltpu.VMEM)] * 2,
        scratch_shapes=[
            pltpu.VMEM((SHARE, 32, WIDTH), bf16),
            pltpu.VMEM((PIECE, HEAD_WIDTH), bf16),
            pltpu.VMEM((SHARE, ROWS, WIDTH), bf16),
            pltpu.VMEM((WIDTH, COLUMNS), bf16),
            pltpu.VMEM((WIDTH, HEADS * HEAD_WIDTH), bf16),
            pltpu.VMEM((GROUPS, SHARE, ROWS, HEAD_WIDTH), bf16),
            pltpu.VMEM((2, SHARE, BACK[0] + ROWS, HEAD_WIDTH), bf16),
            pltpu.VMEM((2, SHARE, BACK[1] + ROWS, HEAD_WIDTH), bf16),
            pltpu.VMEM((2, SHARE, BACK[2] + ROWS, HEAD_WIDTH), bf16),
            pltpu.VMEM((BLOCK, KEYS), f32),
            pltpu.VMEM((SHARE, ROWS, HEAD_WIDTH), bf16),
            pltpu.VMEM((BATCH, 32, HEADS * HEAD_WIDTH), bf16),
            pltpu.VMEM((4, 8, 128), f32),
            pltpu.VMEM((2, 2, 8, 128), f32),
            pltpu.SemaphoreType.DMA((1,)),
            pltpu.SemaphoreType.DMA((TRANSFERS,)),
            pltpu.SemaphoreType.DMA((TRANSFERS,)),
        ],
        compiler_params=pltpu.CompilerParams(
            collective_id=0, has_side_effects=True, vmem_limit_bytes=44 * 1024 * 1024
        ),
    )(
        jnp.transpose(tokens, (1, 0, 2)), norm_gain.reshape(1, WIDTH),
        w_query, w_key, w_value, jnp.transpose(w_out),
    )
    return (jnp.transpose(mixed, (1, 0, 2)), jnp.transpose(logs, (2, 0, 1)))


def solution(mesh):
    in_specs = (
        P(("sp", "tp"), None, None),
        P(),
        P(None, "sp", "tp"),
        P(None, "sp", "tp"),
        P(None, "sp", "tp"),
        P("tp", "sp"),
    )
    out_specs = (P(("sp", "tp"), None, None), P("sp", None, "tp"))
    return jax.shard_map(shards, mesh=mesh, in_specs=in_specs, out_specs=out_specs, check_vma=False)
```

time: 100 us -> 85.5 us (0.85)
  Pallas kernels: 84.4 us -> 77.8 us
  local copies, waits for them, and re-layouts: 10.5 us -> 6.73 us
  other arithmetic: 3.36 us -> 0 us
    pallas_call x1, Pallas kernels: 84.4 us -> 77.8 us  [shards(): pl.pallas_call(kernel, out_shape=(jax.ShapeDtypeStruct((BATCH, 32, WIDTH)...]
    unnamed x25 -> x14, local copies, waits for them, and re-layouts: 9.92 us -> 6.73 us
    reduce_sum x1 -> x0, other arithmetic: 1.44 us -> none  [rms_normed(): jnp.mean(widened * widened, axis=-1, keepdims=True) + epsilon]
    transpose x1 -> x0, other arithmetic: 1.13 us -> none  [shards(): normed = jnp.transpose(rms_normed(tokens, norm_gain), (1, 0, 2))]
where the time goes in v2:
time: 85.5 us; the launch traced here: 85.2 us
  Pallas kernels  77.8 us (91%)
  local copies, waits for them, and re-layouts  6.73 us (8%)
    pallas_call x1, Pallas kernels, shards(): pl.pallas_call(kernel, out_shape=(jax.ShapeDtypeStruct((BATCH, 32, WIDTH)...  77.8 us
    unnamed x14, local copies, waits for them, and re-layouts  6.73 us

profile of v2, /device:TPU:1, one launch (start us, length us, event | category | flops | bytes accessed | tf_op | source)
XLA Modules:
  0.0 85.2 jit_solution(9109709644182154173)
XLA Ops:
  0.6 0.0 copy-start
  0.6 1.1 %copy-done = bf16[32,6,2048]{2,0,1:T(8,128)(2,1)S(1)} copy-done((bf16[32,6,2048]{2,0,1:T(8,128)(2,1)S(1)}, bf16[32,6,2048]{2,0,1:T(8,128)(2,1)}, u32[]{:S(2)}) %copy-start) | copy-done | bytes 786456
  1.8 0.0 copy-start.1
  1.8 0.9 %copy-done.1 = bf16[3,64,256]{2,1,0:T(8,128)(2,1)S(1)} copy-done((bf16[3,64,256]{2,1,0:T(8,128)(2,1)S(1)}, bf16[3,64,256]{2,1,0:T(8,128)(2,1)}, u32[]{:S(2)}) %copy-start.1) | copy-done | bytes 98328
  2.7 0.0 copy-start.2
  2.7 0.9 %copy-done.2 = bf16[3,64,256]{2,1,0:T(8,128)(2,1)S(1)} copy-done((bf16[3,64,256]{2,1,0:T(8,128)(2,1)S(1)}, bf16[3,64,256]{2,1,0:T(8,128)(2,1)}, u32[]{:S(2)}) %copy-start.2) | copy-done | bytes 98328
  3.6 0.0 copy-start.3
  3.6 0.9 %copy-done.3 = bf16[3,64,256]{2,1,0:T(8,128)(2,1)S(1)} copy-done((bf16[3,64,256]{2,1,0:T(8,128)(2,1)S(1)}, bf16[3,64,256]{2,1,0:T(8,128)(2,1)}, u32[]{:S(2)}) %copy-start.3) | copy-done | bytes 98328
  4.4 0.0 copy-start.4
  4.4 0.8 copy-done.4
  5.2 0.0 copy-start.5
  5.2 0.7 copy-done.5
  5.9 77.8 %shard_map.77 = (bf16[6,32,2048]{2,1,0:T(8,128)(2,1)S(1)}, f32[6,2,128]{2,1,0:T(2,128)S(1)}) custom-call(bf16[6,32,2048]{2,1,0:T(8,128)(2,1)S(1)} %bitcast.5, f32[1,2048]{1,0:T(1,128)S(1)} %bitcast.8, bf16[3,64,256]{2,1,0:T(8,128)(2,1)S(1)} %copy-done.1, bf16[3,64,256]{2,1,0:T(8,128)(2,1)S(1)} %copy-done.2, bf16[3,64,256]{2,1,0:T(8,128)(2,1)S(1)} %copy-done.3, ...), custom_call_target="tpu_custom_call" | custom-call | tf_op jit(solution)/shard_map/pallas_call | solution.py:427
  83.7 0.9 %copy.10 = bf16[32,6,2048]{2,0,1:T(8,128)(2,1)} copy(bf16[32,6,2048]{2,0,1:T(8,128)(2,1)S(1)} %bitcast.6) | data formatting | bytes 1572864
  84.6 0.6 copy.11
Async XLA Ops:
  0.6 1.1 %copy-start = (bf16[32,6,2048]{2,0,1:T(8,128)(2,1)S(1)}, bf16[32,6,2048]{2,0,1:T(8,128)(2,1)}, u32[]{:S(2)}) copy-start(bf16[32,6,2048]{2,0,1:T(8,128)(2,1)} %param.6) | copy-start | bytes 2359300
  1.8 0.9 %copy-start.1 = (bf16[3,64,256]{2,1,0:T(8,128)(2,1)S(1)}, bf16[3,64,256]{2,1,0:T(8,128)(2,1)}, u32[]{:S(2)}) copy-start(bf16[3,64,256]{2,1,0:T(8,128)(2,1)} %w_query.1) | copy-start | bytes 294916
  2.7 0.9 %copy-start.2 = (bf16[3,64,256]{2,1,0:T(8,128)(2,1)S(1)}, bf16[3,64,256]{2,1,0:T(8,128)(2,1)}, u32[]{:S(2)}) copy-start(bf16[3,64,256]{2,1,0:T(8,128)(2,1)} %w_key.1) | copy-start | bytes 294916
  3.6 0.9 %copy-start.3 = (bf16[3,64,256]{2,1,0:T(8,128)(2,1)S(1)}, bf16[3,64,256]{2,1,0:T(8,128)(2,1)}, u32[]{:S(2)}) copy-start(bf16[3,64,256]{2,1,0:T(8,128)(2,1)} %w_value.1) | copy-start | bytes 294916
  4.4 0.8 copy-start.4
  5.2 0.7 copy-start.5

commit v3 on v2

v3 whole, which is shorter than its diff:
```python
import functools
import math

import jax
import jax.numpy as jnp
from jax import lax
from jax.experimental import pallas as pl
from jax.experimental.pallas import tpu as pltpu
from jax.sharding import PartitionSpec as P

GROUPS = 3
HEADS = 8
HEAD_WIDTH = 128
STEPS = 24
DILATION_MIDDLE = 4
DILATION_WIDE = 16
WIDTH = 2048
BATCH = 6
SHARE = BATCH // 2
ROWS = 512
AHEAD = (1, 1, 3)
BLOCK = 128
BLOCKS = ROWS // BLOCK
WINDOW = tuple((ahead + 1) * BLOCK for ahead in AHEAD)
KEYS = sum(WINDOW)
PIECE = 64
COLUMNS = 10 * HEAD_WIDTH
UNITS = ((0, 5 * HEAD_WIDTH), (5 * HEAD_WIDTH, 10 * HEAD_WIDTH))
ABSENT = -1e30

epsilon = 1e-06
MESH = pl.DeviceIdType.MESH


def rms_normed(widened, gain):
    scaled = widened * lax.rsqrt(jnp.mean(widened * widened, axis=-1, keepdims=True) + epsilon)
    return (scaled * gain).astype(jnp.bfloat16)


def dot(a, b):
    return lax.dot_general(a, b, (((1,), (0,)), ((), ())), preferred_element_type=jnp.float32)


def dot_t(a, b):
    return lax.dot_general(a, b, (((1,), (1,)), ((), ())), preferred_element_type=jnp.float32)


def kernel(
    tokens, gain, w_query, w_key, w_value, w_out, out, logs,
    raw, gains, gift, toks, weights, whole_out, queries, near, middle, wide, bias,
    combined, arrived, log_rows, both_logs, own_sem, send_sem, recv_sem,
):
    s, x = lax.axis_index("sp"), lax.axis_index("tp")
    core, chip = lax.rem(s, 2), lax.div(s, 2)
    y, z = lax.rem(chip, 4), lax.div(chip, 4)

    def turn(value, by):
        return lax.rem(value + (by + 4), 4)

    def spot(y_at, z_at, core_at):
        return (z_at * 4 + y_at) * 2 + core_at

    zp, zm, xp, xm = (turn(v, d) for v in (z, x) for d in (1, -1))
    line = lax.rem(y, 2)
    pair_y, apart_y = y + 1 - 2 * line, turn(y, 2 * line - 1)
    share = lax.rem(lax.div(y + 1, 2), 2)
    other = 1 - core
    partner = (spot(y, z, other), x)
    z_plus, z_minus = (spot(y, zp, core), x), (spot(y, zm, core), x)
    x_plus, x_minus = (s, xp), (s, xm)
    upper = lax.div(y, 2)
    later = (spot(3 - y, turn(z, upper), core), x)
    head = 2 * x + core

    crowd = []
    for flip_line in (0, 1):
        for flip_core in (0, 1):
            for step in range(4):
                if flip_line or flip_core or step:
                    y_at = pair_y if flip_line else y
                    core_at = other if flip_core else core
                    crowd.append((flip_line, flip_core, step, (spot(y_at, z, core_at), turn(x, step))))
    y_pair, y_apart = (spot(pair_y, z, core), x), (spot(apart_y, z, core), x)
    greeted = [partner, x_plus, x_minus, y_pair, y_apart, z_plus, z_minus]

    barrier = pltpu.get_barrier_semaphore()
    for device in greeted:
        pl.semaphore_signal(barrier, inc=1, device_id=device, device_id_type=MESH)

    counts, opened = [0], [0]

    def tiles_of(ref):
        return math.prod(ref.shape) * ref.dtype.itemsize // 4096

    def shape_of(count):
        for across_at in range(10, 0, -1):
            if count % across_at == 0 and count // across_at <= WIDTH // 16:
                return count // across_at, across_at
        return None

    def extent(count):
        down, over = shape_of(count)
        return weights.at[: down * 16, : over * HEAD_WIDTH]

    class Transfer:
        def __init__(self):
            self.index = opened[0]
            opened[0] += 1
            self.count = 0

        def begin(self, src, dst, device):
            count = tiles_of(src)
            if counts[-1] >= 560 and shape_of(counts[-1]):
                counts.append(0)
            counts[-1] += count
            self.count += count
            pltpu.make_async_remote_copy(
                src_ref=src, dst_ref=dst, send_sem=send_sem.at[len(counts) - 1],
                recv_sem=recv_sem.at[self.index], device_id=device, device_id_type=MESH,
            ).start()

        def arrive(self):
            self.done = True
            whole = extent(self.count)
            pltpu.make_async_copy(whole, whole, recv_sem.at[self.index]).wait()

    def send(src, dst, device):
        transfer = Transfer()
        transfer.begin(src, dst, device)
        return transfer

    def weight_rows(s_at, unit, first=0, count=PIECE):
        left, right = UNITS[unit]
        return weights.at[pl.ds(pl.multiple_of(s_at * PIECE + first, 16), count), left:right]

    def token_rows(line_at, core_at, x_at, b):
        return toks.at[x_at, b, line_at * 2 + core_at]

    take_tokens = pltpu.make_async_copy(tokens, raw, own_sem.at[0])
    take_gain = pltpu.make_async_copy(gain, gains, own_sem.at[1])
    take_tokens.start()
    take_gain.start()
    parts = [(w, group) for group in (2, 1) for w in (w_key, w_value)] + [(w_out, None)]
    parts += [(w_key, 0), (w_value, 0)] + [(w_query, group) for group in (2, 1, 0)]
    rows = pl.ds(pl.multiple_of(s * PIECE, PIECE), PIECE)

    def part_of(index, core_at):
        w, group = parts[index]
        lanes = pl.ds(pl.multiple_of(core_at * HEAD_WIDTH, HEAD_WIDTH), HEAD_WIDTH)
        src = w.at[:, lanes] if group is None else w.at[group, :, lanes]
        return src, weights.at[rows, index * HEAD_WIDTH : (index + 1) * HEAD_WIDTH]

    for index in range(10):
        pltpu.make_async_copy(*part_of(index, core), own_sem.at[2 + index // 5]).start()

    def normed(b):
        return rms_normed(raw[b].astype(jnp.float32), gains[...])

    take_tokens.wait()
    take_gain.wait()
    for b in range(SHARE):
        toks[x, b, line * 2 + core] = normed(share * SHARE + b)
    for b in range(SHARE):
        gift[b] = normed((1 - share) * SHARE + b)

    pl.semaphore_wait(barrier, len(greeted))

    swap = []
    for unit in (0, 1):
        swap.append(Transfer())
        for index in range(5 * unit, 5 * unit + 5):
            src, dst = part_of(index, other)
            swap[unit].begin(src, dst, partner)

    class Ring:
        def __init__(self, rows_of, first, second, cut):
            self.rows_of, self.first, self.second, self.cut = rows_of, first, second, cut
            rows = rows_of(0)
            self.to_second = send(rows, rows, second)
            self.to_first = send(rows, rows, first)

        def onward(self):
            self.from_first_arrive()
            self.from_second_arrive()

    class ZRing(Ring):
        def from_first_arrive(self):
            self.to_second.arrive()
            rows = self.rows_of(-1, self.cut, PIECE - self.cut)
            self.on_second = send(rows, rows, self.second)

        def from_second_arrive(self):
            self.to_first.arrive()
            rows = self.rows_of(1, 0, self.cut)
            self.on_first = send(rows, rows, self.first)

        def far(self):
            self.on_second.arrive()
            self.on_first.arrive()

    class YRing(ZRing):
        def from_first_arrive(self):
            self.to_first.arrive()
            rows = self.rows_of("pair", self.cut, PIECE - self.cut)
            self.on_second = send(rows, rows, self.second)

        def from_second_arrive(self):
            self.to_second.arrive()
            rows = self.rows_of("apart", 0, self.cut)
            self.on_first = send(rows, rows, self.first)

    ys = {0: y, "pair": pair_y, "apart": apart_y, "far": turn(y, 2)}

    def y_ring(dz, core_at, unit):
        return YRing(
            lambda step, *cut: weight_rows(spot(ys[step], turn(z, dz), core_at), unit, *cut),
            y_pair, y_apart, 48,
        )

    def z_ring(dy, core_at, unit):
        return ZRing(
            lambda step, *cut: weight_rows(spot(ys[dy], turn(z, step), core_at), unit, *cut),
            z_minus, z_plus, 48,
        )

    across = {step: Transfer() for step in (0, -1, 1, 2)}
    give = [None] * SHARE

    def token_steps():
        up, down, far_up, far_down = {}, {}, {}, {}

        def cross(step, line_at, b):
            rows = token_rows(line_at, core, turn(x, step), b)
            across[step].begin(rows, rows, partner)

        def launch(line_at, b):
            rows = token_rows(line_at, core, x, b)
            which = 0 if line_at is line else 1
            up[which, b] = send(rows, rows, x_plus)
            down[which, b] = send(rows, rows, x_minus)
            cross(0, line_at, b)

        def onward(which, step, b):
            line_at = (line, far_line)[which]
            (up if step == -1 else down)[which, b].arrive()
            if (which, step) in ((0, -1), (1, 1)):
                rows = token_rows(line_at, core, turn(x, step), b)
                if step == -1:
                    far_up[b] = send(rows, rows, x_plus)
                else:
                    far_down[b] = send(rows, rows, x_minus)
            cross(step, line_at, b)

        far_line = 1 - line
        for b in range(SHARE):
            launch(line, b)
        yield
        for b in range(SHARE):
            give[b].arrive()
            launch(far_line, b)
            yield
        for b in range(SHARE):
            onward(0, -1, b)
            onward(0, 1, b)
            yield
        for b in range(SHARE):
            onward(1, 1, b)
            onward(1, -1, b)
            yield
        for b in range(SHARE):
            far_up[b].arrive()
            cross(2, line, b)
            far_down[b].arrive()
            cross(2, far_line, b)
            yield

    def weight_steps(unit):
        own, their = {}, {}
        whole = weight_rows(s, unit)
        pltpu.make_async_copy(whole, whole, own_sem.at[2 + unit]).wait()
        own["first"] = y_ring(0, core, unit)
        own[0] = z_ring(0, core, unit)
        yield
        swap[unit].arrive()
        their["first"] = z_ring(0, other, unit)
        their[0] = y_ring(0, other, unit)
        yield
        own["first"].onward()
        own["pair"] = z_ring("pair", core, unit)
        own["apart"] = z_ring("apart", core, unit)
        own[0].onward()
        yield
        their["first"].onward()
        their[-1] = y_ring(-1, other, unit)
        their[1] = y_ring(1, other, unit)
        their[0].onward()
        yield
        own["first"].far()
        own["far"] = z_ring("far", core, unit)
        their["first"].far()
        their[2] = y_ring(2, other, unit)
        yield
        for y_step, z_step in (("pair", -1), ("apart", 1)):
            own[y_step].onward()
            their[z_step].onward()
            yield
        own["far"].onward()
        their[2].onward()
        yield
        for y_step, z_step in zip(ys, (0, -1, 1, 2)):
            own[y_step].far()
            their[z_step].far()
        yield

    steps = {"t": token_steps(), "0": weight_steps(0), "1": weight_steps(1)}

    def go(order):
        for which in order.replace(" ", ""):
            next(steps[which])

    give[0] = send(gift.at[0], token_rows(line, core, x, 0), y_pair)
    go("0t")
    give[1] = send(gift.at[1], token_rows(line, core, x, 1), y_pair)
    go("01")
    give[2] = send(gift.at[2], token_rows(line, core, x, 2), y_pair)

    near[:, :, 0, :96, :] = jnp.zeros((2, SHARE, 96, HEAD_WIDTH), jnp.bfloat16)
    log_rows[...] = jnp.zeros_like(log_rows)
    left = 0
    for ahead, window, dilation in zip(AHEAD, WINDOW, (1, DILATION_MIDDLE, DILATION_WIDE)):
        query_at = lax.broadcasted_iota(jnp.int32, (BLOCK, window), 0)
        key_at = lax.broadcasted_iota(jnp.int32, (BLOCK, window), 1)
        lag = query_at + ahead * BLOCK - key_at
        allowed = (lag >= 0) & (lag <= STEPS * dilation) & ((lag & (dilation - 1)) == 0)
        bias[:, left : left + window] = jnp.where(allowed, jnp.float32(0), jnp.float32(ABSENT))
        left += window

    def project(x_at, left, width):
        rows = toks[x_at].reshape(SHARE * BLOCKS * 32, WIDTH)
        return dot(rows, weights[:, left : left + width]).astype(jnp.bfloat16)

    def block_rows(x_at):
        return pl.ds(pl.multiple_of(x_at * 32, 32), 32)

    def lay(found, left, buffer, x_at, ahead):
        part = found[:, left : left + HEAD_WIDTH].reshape(SHARE, BLOCKS, 32, HEAD_WIDTH)
        buffer[:, ahead : ahead + BLOCKS, block_rows(x_at), :] = part

    def keys_of(step):
        x_at = turn(x, step)
        across[step].arrive()
        for place, (keys, group) in enumerate(((wide, 2), (middle, 1))):
            found = project(x_at, place * 2 * HEAD_WIDTH, 2 * HEAD_WIDTH)
            for which in (0, 1):
                lay(found, which * HEAD_WIDTH, keys.at[which], x_at, AHEAD[group])

    halo = []

    def pass_on(keys, group, x_at, share_at):
        ahead = AHEAD[group]
        halo.append(
            send(
                keys.at[:, share_at, BLOCKS:, block_rows(x_at), :],
                keys.at[:, share_at, :ahead, block_rows(x_at), :],
                later,
            )
        )

    def pass_all(step):
        for keys, group in ((wide, 2), (middle, 1)):
            pass_on(keys, group, turn(x, step), slice(None))

    def head_columns(x_at, core_at, half=None):
        lanes = pl.ds(pl.multiple_of((2 * x_at + core_at) * HEAD_WIDTH, HEAD_WIDTH), HEAD_WIDTH)
        if half is None:
            return whole_out.at[:, lanes]
        return whole_out.at[pl.ds(half * (WIDTH // 2), WIDTH // 2), lanes]

    out_swap = []

    def out_steps():
        out_rows = weights.at[:, 4 * HEAD_WIDTH : 5 * HEAD_WIDTH]
        mine = head_columns(x, core)
        up = send(out_rows, mine, x_plus)
        down = send(out_rows, mine, x_minus)
        out_swap.append(send(out_rows, mine, partner))
        lanes = pl.ds(pl.multiple_of(head * HEAD_WIDTH, HEAD_WIDTH), HEAD_WIDTH)
        whole_out[:, lanes] = weights[:, 4 * HEAD_WIDTH : 5 * HEAD_WIDTH]
        yield
        up.arrive()
        rows = head_columns(xm, core, 0)
        far_up = send(rows, rows, x_plus)
        rows = head_columns(xm, core)
        out_swap.append(send(rows, rows, partner))
        down.arrive()
        rows = head_columns(xp, core, 1)
        far_down = send(rows, rows, x_minus)
        rows = head_columns(xp, core)
        out_swap.append(send(rows, rows, partner))
        yield
        far_up.arrive()
        rows = head_columns(turn(x, 2), core, 0)
        out_swap.append(send(rows, rows, partner))
        far_down.arrive()
        rows = head_columns(turn(x, 2), core, 1)
        out_swap.append(send(rows, rows, partner))
        yield

    steps["o"] = out_steps()

    go("00t1t0t1t0t10t100tt")
    keys_of(0)
    pass_all(0)
    go("1to11")
    keys_of(-1)
    pass_all(-1)
    keys_of(1)
    pass_all(1)
    go("ttt")
    keys_of(2)
    for b in range(SHARE):
        for keys, group in ((wide, 2), (middle, 1)):
            pass_on(keys, group, turn(x, 2), pl.ds(b, 1))
    go("1")

    def keys_near(x_at, carry):
        found = project(x_at, UNITS[1][0], 2 * HEAD_WIDTH)
        for which in (0, 1):
            lay(found, which * HEAD_WIDTH, near.at[which], x_at, AHEAD[0])
        return carry

    lax.fori_loop(0, 4, keys_near, 0)
    near_halo = send(near.at[:, :, BLOCKS, 96:, :], near.at[:, :, 0, 96:, :], later)

    def ask(x_at, carry):
        left = UNITS[1][0] + 2 * HEAD_WIDTH
        found = project(x_at, left, 2 * HEAD_WIDTH)
        lay(found, 0, queries.at[2], x_at, 0)
        lay(found, HEAD_WIDTH, queries.at[1], x_at, 0)
        lay(project(x_at, left + 2 * HEAD_WIDTH, HEAD_WIDTH), 0, queries.at[0], x_at, 0)
        return carry

    lax.fori_loop(0, 4, ask, 0)

    factor = math.log2(math.e) / math.sqrt(HEAD_WIDTH)
    start_at = (z * 2 + upper) * ROWS
    lanes = pl.ds(pl.multiple_of(head * HEAD_WIDTH, HEAD_WIDTH), HEAD_WIDTH)

    def attend(b, block):
        scores, left = [], 0
        for group, keys in enumerate((near, middle, wide)):
            window = WINDOW[group]
            seen = keys[0, b, block : block + AHEAD[group] + 1].reshape(window, HEAD_WIDTH)
            score = dot_t(queries[group, b, block], seen)
            first = start_at + (block - AHEAD[group]) * BLOCK
            hidden = bias[:, left : left + window]
            if block < AHEAD[group]:
                key_at = lax.broadcasted_iota(jnp.int32, (1, window), 1) + first
                hidden = hidden + jnp.where(key_at >= 0, jnp.float32(0), jnp.float32(ABSENT))
            scores.append(score * factor + hidden)
            left += window
        peak = functools.reduce(
            jnp.maximum, [jnp.max(score, axis=1, keepdims=True) for score in scores]
        )
        total, mixed = 0.0, 0.0
        for group, keys in enumerate((near, middle, wide)):
            lifted = jnp.exp2(scores[group] - peak)
            total = total + jnp.sum(lifted, axis=1, keepdims=True)
            seen = keys[1, b, block : block + AHEAD[group] + 1].reshape(WINDOW[group], HEAD_WIDTH)
            mixed = mixed + dot(lifted.astype(jnp.bfloat16), seen)
        combined[b, block * BLOCK : (block + 1) * BLOCK, :] = (mixed / total).astype(jnp.bfloat16)
        log = (peak + jnp.log2(total)) * math.log(2.0)
        log_rows[block, b : b + 1, :] = jnp.transpose(jnp.broadcast_to(log, (BLOCK, BLOCK)))[0:1, :]

    def rows_for(line_at, core_at, x_at):
        return pl.ds(pl.multiple_of(line_at * 256 + core_at * 128 + x_at * 32, 32), 32)

    for b in range(SHARE):
        attend(b, BLOCKS - 1)
    go("o")
    near_halo.arrive()
    for copy in halo[:6]:
        copy.arrive()
    exchange = Transfer()
    for b in range(SHARE):
        halo[6 + 2 * b].arrive()
        halo[7 + 2 * b].arrive()
        for block in range(BLOCKS - 1):
            attend(b, block)

        for flip_line, flip_core, step, device in crowd:
            line_at = 1 - line if flip_line else line
            core_at = other if flip_core else core
            exchange.begin(
                combined.at[b, rows_for(line_at, core_at, turn(x, step)), :],
                arrived.at[share * SHARE + b, :, lanes],
                device,
            )
            if step == 0 and b == SHARE - 1:
                exchange.begin(
                    log_rows.at[line_at * 2 + core_at], both_logs.at[core, share], device
                )
        arrived[share * SHARE + b, :, lanes] = combined[b, rows_for(line, core, x), :]
        if b == 0:
            go("o")
    both_logs[core, share] = log_rows[line * 2 + core]
    for copy in out_swap + [exchange]:
        copy.arrive()

    everything = arrived[...].reshape(192, HEADS * HEAD_WIDTH)
    for tile in range(8):
        part = dot_t(everything, whole_out[tile * 256 : (tile + 1) * 256, :]).astype(jnp.bfloat16)
        out[:, :, tile * 256 : (tile + 1) * 256] = part.reshape(BATCH, 32, 256)
    for core_at in range(2):
        for share_at in range(2):
            for b in range(SHARE):
                logs[share_at * SHARE + b, core_at : core_at + 1, :] = both_logs[core_at, share_at, b : b + 1, :]

    assert opened[0] <= ARRIVALS and len(counts) <= SENDS, (opened, counts)
    for index, count in enumerate(counts):
        whole = extent(count)
        pltpu.make_async_copy(whole, whole, send_sem.at[index]).wait()


ARRIVALS = 130
SENDS = 8


def shards(tokens, norm_gain, w_query, w_key, w_value, w_out):
    bf16, f32 = jnp.bfloat16, jnp.float32
    operands = (
        jnp.transpose(tokens, (1, 0, 2)), norm_gain.reshape(1, WIDTH),
        w_query, w_key, w_value, jnp.transpose(w_out),
    )
    mixed, logs = pl.pallas_call(
        kernel,
        out_shape=(
            jax.ShapeDtypeStruct((BATCH, 32, WIDTH), bf16),
            jax.ShapeDtypeStruct((BATCH, 2, 128), f32),
        ),
        in_specs=[pl.BlockSpec(memory_space=pltpu.HBM)] * 6,
        out_specs=[pl.BlockSpec(memory_space=pltpu.VMEM)] * 2,
        scratch_shapes=[
            pltpu.VMEM((BATCH, 32, WIDTH), bf16),
            pltpu.VMEM((1, WIDTH), f32),
            pltpu.VMEM((SHARE, 32, WIDTH), bf16),
            pltpu.VMEM((4, SHARE, BLOCKS, 32, WIDTH), bf16),
            pltpu.VMEM((WIDTH, COLUMNS), bf16),
            pltpu.VMEM((WIDTH, HEADS * HEAD_WIDTH), bf16),
            pltpu.VMEM((GROUPS, SHARE, BLOCKS, BLOCK, HEAD_WIDTH), bf16),
            pltpu.VMEM((2, SHARE, AHEAD[0] + BLOCKS, BLOCK, HEAD_WIDTH), bf16),
            pltpu.VMEM((2, SHARE, AHEAD[1] + BLOCKS, BLOCK, HEAD_WIDTH), bf16),
            pltpu.VMEM((2, SHARE, AHEAD[2] + BLOCKS, BLOCK, HEAD_WIDTH), bf16),
            pltpu.VMEM((BLOCK, KEYS), f32),
            pltpu.VMEM((SHARE, ROWS, HEAD_WIDTH), bf16),
            pltpu.VMEM((BATCH, 32, HEADS * HEAD_WIDTH), bf16),
            pltpu.VMEM((4, 8, 128), f32),
            pltpu.VMEM((2, 2, 8, 128), f32),
            pltpu.SemaphoreType.DMA((4,)),
            pltpu.SemaphoreType.DMA((SENDS,)),
            pltpu.SemaphoreType.DMA((ARRIVALS,)),
        ],
        compiler_params=pltpu.CompilerParams(
            collective_id=0, has_side_effects=True, vmem_limit_bytes=44 * 1024 * 1024
        ),
    )(*(pltpu.with_memory_space_constraint(array, pltpu.HBM) for array in operands))
    return (jnp.transpose(mixed, (1, 0, 2)), jnp.transpose(logs, (2, 0, 1)))


def solution(mesh):
    in_specs = (
        P(("sp", "tp"), None, None),
        P(),
        P(None, "sp", "tp"),
        P(None, "sp", "tp"),
        P(None, "sp", "tp"),
        P("tp", "sp"),
    )
    out_specs = (P(("sp", "tp"), None, None), P("sp", None, "tp"))
    return jax.shard_map(shards, mesh=mesh, in_specs=in_specs, out_specs=out_specs, check_vma=False)
```

time: 85.5 us -> 83.5 us (0.977)
  local copies, waits for them, and re-layouts: 6.73 us -> 1.47 us
  Pallas kernels: 77.8 us -> 81.3 us
    unnamed x14 -> x2, local copies, waits for them, and re-layouts: 6.73 us -> 1.47 us
    pallas_call x1, Pallas kernels: 77.8 us -> 81.3 us  [shards(): pl.pallas_call(kernel, out_shape=(jax.ShapeDtypeStruct((BATCH, 32, WIDTH)...]
where the time goes in v3:
time: 83.5 us; the launch traced here: 83.4 us
  Pallas kernels  81.3 us (97%)
  local copies, waits for them, and re-layouts  1.47 us (2%)
    pallas_call x1, Pallas kernels, shards(): pl.pallas_call(kernel, out_shape=(jax.ShapeDtypeStruct((BATCH, 32, WIDTH)...  81.3 us

profile of v3, /device:TPU:1, one launch (start us, length us, event | category | flops | bytes accessed | tf_op | source)
XLA Modules:
  0.0 83.4 jit_solution(17658694843462245142)
XLA Ops:
  0.6 81.3 %shard_map.77 = (bf16[6,32,2048]{2,1,0:T(8,128)(2,1)S(1)}, f32[6,2,128]{2,1,0:T(2,128)S(1)}) custom-call(bf16[6,32,2048]{2,1,0:T(8,128)(2,1)} %bitcast.7, f32[1,2048]{1,0:T(1,128)} %bitcast.9, bf16[3,64,256]{2,1,0:T(8,128)(2,1)} %w_query.1, bf16[3,64,256]{2,1,0:T(8,128)(2,1)} %w_key.1, bf16[3,64,256]{2,1,0:T(8,128)(2,1)} %w_value.1, bf16[64,256]{1,0:T(8,128)(2,1)} %bitcast.8), custom_call_target="tpu_custom_call" | custom-call | tf_op jit(solution)/shard_map/pallas_call | solution.py:535
  81.9 0.9 %copy.10 = bf16[32,6,2048]{2,0,1:T(8,128)(2,1)} copy(bf16[32,6,2048]{2,0,1:T(8,128)(2,1)S(1)} %bitcast.5) | data formatting | bytes 1572864
  82.8 0.6 copy.11

commit v4 on v3

--- a/solution.py
+++ b/solution.py
@@ -27,6 +27,18 @@
 COLUMNS = 10 * HEAD_WIDTH
 UNITS = ((0, 5 * HEAD_WIDTH), (5 * HEAD_WIDTH, 10 * HEAD_WIDTH))
 ABSENT = -1e30
+ORDER = (
+    "t00", "O0", "G0", "t01", "t02", "R0", "G1", "G2", "Op0", "Oa0", "Zm00", "Zp00", "up00",
+    "dn00", "Rm0", "Rp0", "Ya00", "g0", "up01", "dn01", "Zmp0", "Zpp0", "Yp00", "Zma0",
+    "Zpa0", "Yam0", "O1", "up02", "dn02", "g1", "Rf0", "Yap0", "dn10", "fu0", "R1", "Of0",
+    "g2", "Zm01", "Zp01", "Oa1", "Ypm0", "up10", "dn11", "Yaf0", "Ypp0", "Rm1", "fu1", "Rp1",
+    "fd0", "Zmf0", "Zpf0", "Op1", "Ya01", "Ypf0", "fu2", "dn12", "Zma1", "Zpa1", "Yp01",
+    "Rf1", "Yam1", "up11", "fd1", "Of1", "Yap1", "Zmp1", "Zpp1", "Ypm1", "W0", "o0", "K0",
+    "up12", "fd2", "Ypp1", "Yaf1", "Zmf1", "Zpf1", "Km", "Ypf1", "Kp", "K2", "W1", "N", "oum",
+    "odm", "Q",
+)
+Y_CUT = (0, 64)
+Z_CUT = (32, 32)
 
 epsilon = 1e-06
 MESH = pl.DeviceIdType.MESH
@@ -110,7 +122,7 @@
 
         def begin(self, src, dst, device):
             count = tiles_of(src)
-            if counts[-1] >= 560 and shape_of(counts[-1]):
+            if counts[-1] >= 520 and shape_of(counts[-1]):
                 counts.append(0)
             counts[-1] += count
             self.count += count
@@ -173,156 +185,244 @@
             swap[unit].begin(src, dst, partner)
 
     class Ring:
-        def __init__(self, rows_of, first, second, cut):
+        def __init__(self, rows_of, first, second, names, cut):
             self.rows_of, self.first, self.second, self.cut = rows_of, first, second, cut
+            self.names = names
             rows = rows_of(0)
-            self.to_second = send(rows, rows, second)
-            self.to_first = send(rows, rows, first)
-
-        def onward(self):
-            self.from_first_arrive()
-            self.from_second_arrive()
-
-    class ZRing(Ring):
-        def from_first_arrive(self):
-            self.to_second.arrive()
-            rows = self.rows_of(-1, self.cut, PIECE - self.cut)
-            self.on_second = send(rows, rows, self.second)
-
-        def from_second_arrive(self):
-            self.to_first.arrive()
-            rows = self.rows_of(1, 0, self.cut)
-            self.on_first = send(rows, rows, self.first)
+            to_second, to_first = send(rows, rows, second), send(rows, rows, first)
+            along_y = names[0] == "pair"
+            self.from_first = to_first if along_y else to_second
+            self.from_second = to_second if along_y else to_first
+            self.on = []
+
+        def pass_first(self):
+            self.from_first.arrive()
+            if self.cut < PIECE:
+                rows = self.rows_of(self.names[0], self.cut, PIECE - self.cut)
+                self.on.append(send(rows, rows, self.second))
+
+        def pass_second(self):
+            self.from_second.arrive()
+            if self.cut > 0:
+                rows = self.rows_of(self.names[1], 0, self.cut)
+                self.on.append(send(rows, rows, self.first))
 
         def far(self):
-            self.on_second.arrive()
-            self.on_first.arrive()
-
-    class YRing(ZRing):
-        def from_first_arrive(self):
-            self.to_first.arrive()
-            rows = self.rows_of("pair", self.cut, PIECE - self.cut)
-            self.on_second = send(rows, rows, self.second)
-
-        def from_second_arrive(self):
-            self.to_second.arrive()
-            rows = self.rows_of("apart", 0, self.cut)
-            self.on_first = send(rows, rows, self.first)
+            for copy in self.on:
+                copy.arrive()
 
     ys = {0: y, "pair": pair_y, "apart": apart_y, "far": turn(y, 2)}
+    zs = {0: z, -1: zm, 1: zp, 2: turn(z, 2)}
 
     def y_ring(dz, core_at, unit):
-        return YRing(
-            lambda step, *cut: weight_rows(spot(ys[step], turn(z, dz), core_at), unit, *cut),
-            y_pair, y_apart, 48,
+        return Ring(
+            lambda step, *cut: weight_rows(spot(ys[step], zs[dz], core_at), unit, *cut),
+            y_pair, y_apart, ("pair", "apart"), Y_CUT[unit],
         )
 
     def z_ring(dy, core_at, unit):
-        return ZRing(
-            lambda step, *cut: weight_rows(spot(ys[dy], turn(z, step), core_at), unit, *cut),
-            z_minus, z_plus, 48,
+        return Ring(
+            lambda step, *cut: weight_rows(spot(ys[dy], zs[step], core_at), unit, *cut),
+            z_minus, z_plus, (-1, 1), Z_CUT[unit],
         )
 
+    events = {}
+
     across = {step: Transfer() for step in (0, -1, 1, 2)}
-    give = [None] * SHARE
-
-    def token_steps():
-        up, down, far_up, far_down = {}, {}, {}, {}
-
-        def cross(step, line_at, b):
-            rows = token_rows(line_at, core, turn(x, step), b)
-            across[step].begin(rows, rows, partner)
-
-        def launch(line_at, b):
-            rows = token_rows(line_at, core, x, b)
-            which = 0 if line_at is line else 1
-            up[which, b] = send(rows, rows, x_plus)
-            down[which, b] = send(rows, rows, x_minus)
-            cross(0, line_at, b)
-
-        def onward(which, step, b):
-            line_at = (line, far_line)[which]
-            (up if step == -1 else down)[which, b].arrive()
-            if (which, step) in ((0, -1), (1, 1)):
-                rows = token_rows(line_at, core, turn(x, step), b)
-                if step == -1:
-                    far_up[b] = send(rows, rows, x_plus)
-                else:
-                    far_down[b] = send(rows, rows, x_minus)
-            cross(step, line_at, b)
-
-        far_line = 1 - line
-        for b in range(SHARE):
-            launch(line, b)
-        yield
-        for b in range(SHARE):
+    lines = (line, 1 - line)
+    give, up, down, far_up, far_down = {}, {}, {}, {}, {}
+
+    def cross(step, which, b):
+        rows = token_rows(lines[which], core, turn(x, step), b)
+        across[step].begin(rows, rows, partner)
+
+    def launch(which, b):
+        if which == 1:
             give[b].arrive()
-            launch(far_line, b)
-            yield
-        for b in range(SHARE):
-            onward(0, -1, b)
-            onward(0, 1, b)
-            yield
-        for b in range(SHARE):
-            onward(1, 1, b)
-            onward(1, -1, b)
-            yield
-        for b in range(SHARE):
-            far_up[b].arrive()
-            cross(2, line, b)
-            far_down[b].arrive()
-            cross(2, far_line, b)
-            yield
-
-    def weight_steps(unit):
-        own, their = {}, {}
-        whole = weight_rows(s, unit)
-        pltpu.make_async_copy(whole, whole, own_sem.at[2 + unit]).wait()
-        own["first"] = y_ring(0, core, unit)
-        own[0] = z_ring(0, core, unit)
-        yield
-        swap[unit].arrive()
-        their["first"] = z_ring(0, other, unit)
-        their[0] = y_ring(0, other, unit)
-        yield
-        own["first"].onward()
-        own["pair"] = z_ring("pair", core, unit)
-        own["apart"] = z_ring("apart", core, unit)
-        own[0].onward()
-        yield
-        their["first"].onward()
-        their[-1] = y_ring(-1, other, unit)
-        their[1] = y_ring(1, other, unit)
-        their[0].onward()
-        yield
-        own["first"].far()
-        own["far"] = z_ring("far", core, unit)
-        their["first"].far()
-        their[2] = y_ring(2, other, unit)
-        yield
-        for y_step, z_step in (("pair", -1), ("apart", 1)):
-            own[y_step].onward()
-            their[z_step].onward()
-            yield
-        own["far"].onward()
-        their[2].onward()
-        yield
-        for y_step, z_step in zip(ys, (0, -1, 1, 2)):
-            own[y_step].far()
-            their[z_step].far()
-        yield
-
-    steps = {"t": token_steps(), "0": weight_steps(0), "1": weight_steps(1)}
-
-    def go(order):
-        for which in order.replace(" ", ""):
-            next(steps[which])
-
-    give[0] = send(gift.at[0], token_rows(line, core, x, 0), y_pair)
-    go("0t")
-    give[1] = send(gift.at[1], token_rows(line, core, x, 1), y_pair)
-    go("01")
-    give[2] = send(gift.at[2], token_rows(line, core, x, 2), y_pair)
+        rows = token_rows(lines[which], core, x, b)
+        up[which, b] = send(rows, rows, x_plus)
+        down[which, b] = send(rows, rows, x_minus)
+        cross(0, which, b)
+
+    def onward(which, step, b):
+        (up if step == -1 else down)[which, b].arrive()
+        rows = token_rows(lines[which], core, turn(x, step), b)
+        if (which, step) == (0, -1):
+            far_up[b] = send(rows, rows, x_plus)
+        if (which, step) == (1, 1):
+            far_down[b] = send(rows, rows, x_minus)
+        cross(step, which, b)
+
+    def arrive_far(which, b):
+        (far_up, far_down)[which][b].arrive()
+        cross(2, which, b)
+
+    def present(b):
+        give[b] = send(gift.at[b], token_rows(line, core, x, b), y_pair)
+
+    for b in range(SHARE):
+        events[f"G{b}"] = functools.partial(present, b)
+        for which in (0, 1):
+            events[f"t0{b}" if which == 0 else f"g{b}"] = functools.partial(launch, which, b)
+            events[f"up{which}{b}"] = functools.partial(onward, which, -1, b)
+            events[f"dn{which}{b}"] = functools.partial(onward, which, 1, b)
+            events[f"fu{b}" if which == 0 else f"fd{b}"] = functools.partial(arrive_far, which, b)
+
+    def weight_events(unit):
+        rings = {}
+
+        def event(name):
+            def keep(work):
+                events[name + str(unit)] = work
+            return keep
+
+        def over_z(letter, dy):
+            ring = rings["z" + letter] = z_ring(dy, core, unit)
+            events[f"Zm{letter}{unit}"], events[f"Zp{letter}{unit}"] = ring.pass_first, ring.pass_second
+
+        def over_y(letter, dz):
+            ring = rings["y" + letter] = y_ring(dz, other, unit)
+            events[f"Yp{letter}{unit}"], events[f"Ya{letter}{unit}"] = ring.pass_first, ring.pass_second
+
+        @event("O")
+        def _():
+            whole = weight_rows(s, unit)
+            pltpu.make_async_copy(whole, whole, own_sem.at[2 + unit]).wait()
+            rings["O"] = y_ring(0, core, unit)
+            over_z("0", 0)
+
+        @event("R")
+        def _():
+            swap[unit].arrive()
+            rings["R"] = z_ring(0, other, unit)
+            over_y("0", 0)
+
+        @event("Op")
+        def _():
+            rings["O"].pass_first()
+            over_z("p", "pair")
+
+        @event("Oa")
+        def _():
+            rings["O"].pass_second()
+            over_z("a", "apart")
+
+        @event("Of")
+        def _():
+            rings["O"].far()
+            over_z("f", "far")
+
+        @event("Rm")
+        def _():
+            rings["R"].pass_first()
+            over_y("m", -1)
+
+        @event("Rp")
+        def _():
+            rings["R"].pass_second()
+            over_y("p", 1)
+
+        @event("Rf")
+        def _():
+            rings["R"].far()
+            over_y("f", 2)
+
+        @event("W")
+        def _():
+            for letter in "0paf":
+                rings["z" + letter].far()
+            for letter in "0mpf":
+                rings["y" + letter].far()
+
+    weight_events(0)
+    weight_events(1)
+
+    def project(x_at, left, width):
+        rows = toks[x_at].reshape(SHARE * BLOCKS * 32, WIDTH)
+        return dot(rows, weights[:, left : left + width]).astype(jnp.bfloat16)
+
+    def block_rows(x_at):
+        return pl.ds(pl.multiple_of(x_at * 32, 32), 32)
+
+    def lay(found, left, buffer, x_at, ahead):
+        part = found[:, left : left + HEAD_WIDTH].reshape(SHARE, BLOCKS, 32, HEAD_WIDTH)
+        buffer[:, ahead : ahead + BLOCKS, block_rows(x_at), :] = part
+
+    def keys_of(step):
+        x_at = turn(x, step)
+        across[step].arrive()
+        for place, (keys, group) in enumerate(((wide, 2), (middle, 1))):
+            found = project(x_at, place * 2 * HEAD_WIDTH, 2 * HEAD_WIDTH)
+            for which in (0, 1):
+                lay(found, which * HEAD_WIDTH, keys.at[which], x_at, AHEAD[group])
+
+    halo = []
+
+    def pass_on(keys, group, x_at, share_at):
+        ahead = AHEAD[group]
+        halo.append(
+            send(
+                keys.at[:, share_at, BLOCKS:, block_rows(x_at), :],
+                keys.at[:, share_at, :ahead, block_rows(x_at), :],
+                later,
+            )
+        )
+
+    def pass_all(step):
+        for keys, group in ((wide, 2), (middle, 1)):
+            pass_on(keys, group, turn(x, step), slice(None))
+
+    def head_columns(x_at, core_at, half=None):
+        lanes = pl.ds(pl.multiple_of((2 * x_at + core_at) * HEAD_WIDTH, HEAD_WIDTH), HEAD_WIDTH)
+        if half is None:
+            return whole_out.at[:, lanes]
+        return whole_out.at[pl.ds(half * (WIDTH // 2), WIDTH // 2), lanes]
+
+    out_swap = []
+
+    out_way = {}
+
+    def out_event(name):
+        def keep(work):
+            events[name] = work
+        return keep
+
+    def out_cross(rows):
+        out_swap.append(send(rows, rows, partner))
+
+    @out_event("o0")
+    def _():
+        out_rows = weights.at[:, 4 * HEAD_WIDTH : 5 * HEAD_WIDTH]
+        mine = head_columns(x, core)
+        out_way["up"] = send(out_rows, mine, x_plus)
+        out_way["down"] = send(out_rows, mine, x_minus)
+        out_swap.append(send(out_rows, mine, partner))
+        lanes = pl.ds(pl.multiple_of(head * HEAD_WIDTH, HEAD_WIDTH), HEAD_WIDTH)
+        whole_out[:, lanes] = weights[:, 4 * HEAD_WIDTH : 5 * HEAD_WIDTH]
+
+    @out_event("oum")
+    def _():
+        out_way["up"].arrive()
+        rows = head_columns(xm, core, 0)
+        out_way["far_up"] = send(rows, rows, x_plus)
+        out_cross(head_columns(xm, core))
+
+    @out_event("odm")
+    def _():
+        out_way["down"].arrive()
+        rows = head_columns(xp, core, 1)
+        out_way["far_down"] = send(rows, rows, x_minus)
+        out_cross(head_columns(xp, core))
+
+    @out_event("ofu")
+    def _():
+        out_way["far_up"].arrive()
+        out_cross(head_columns(turn(x, 2), core, 0))
+
+    @out_event("ofd")
+    def _():
+        out_way["far_down"].arrive()
+        out_cross(head_columns(turn(x, 2), core, 1))
 
     near[:, :, 0, :96, :] = jnp.zeros((2, SHARE, 96, HEAD_WIDTH), jnp.bfloat16)
     log_rows[...] = jnp.zeros_like(log_rows)
@@ -335,102 +435,11 @@
         bias[:, left : left + window] = jnp.where(allowed, jnp.float32(0), jnp.float32(ABSENT))
         left += window
 
-    def project(x_at, left, width):
-        rows = toks[x_at].reshape(SHARE * BLOCKS * 32, WIDTH)
-        return dot(rows, weights[:, left : left + width]).astype(jnp.bfloat16)
-
-    def block_rows(x_at):
-        return pl.ds(pl.multiple_of(x_at * 32, 32), 32)
-
-    def lay(found, left, buffer, x_at, ahead):
-        part = found[:, left : left + HEAD_WIDTH].reshape(SHARE, BLOCKS, 32, HEAD_WIDTH)
-        buffer[:, ahead : ahead + BLOCKS, block_rows(x_at), :] = part
-
-    def keys_of(step):
-        x_at = turn(x, step)
-        across[step].arrive()
-        for place, (keys, group) in enumerate(((wide, 2), (middle, 1))):
-            found = project(x_at, place * 2 * HEAD_WIDTH, 2 * HEAD_WIDTH)
-            for which in (0, 1):
-                lay(found, which * HEAD_WIDTH, keys.at[which], x_at, AHEAD[group])
-
-    halo = []
-
-    def pass_on(keys, group, x_at, share_at):
-        ahead = AHEAD[group]
-        halo.append(
-            send(
-                keys.at[:, share_at, BLOCKS:, block_rows(x_at), :],
-                keys.at[:, share_at, :ahead, block_rows(x_at), :],
-                later,
-            )
-        )
-
-    def pass_all(step):
-        for keys, group in ((wide, 2), (middle, 1)):
-            pass_on(keys, group, turn(x, step), slice(None))
-
-    def head_columns(x_at, core_at, half=None):
-        lanes = pl.ds(pl.multiple_of((2 * x_at + core_at) * HEAD_WIDTH, HEAD_WIDTH), HEAD_WIDTH)
-        if half is None:
-            return whole_out.at[:, lanes]
-        return whole_out.at[pl.ds(half * (WIDTH // 2), WIDTH // 2), lanes]
-
-    out_swap = []
-
-    def out_steps():
-        out_rows = weights.at[:, 4 * HEAD_WIDTH : 5 * HEAD_WIDTH]
-        mine = head_columns(x, core)
-        up = send(out_rows, mine, x_plus)
-        down = send(out_rows, mine, x_minus)
-        out_swap.append(send(out_rows, mine, partner))
-        lanes = pl.ds(pl.multiple_of(head * HEAD_WIDTH, HEAD_WIDTH), HEAD_WIDTH)
-        whole_out[:, lanes] = weights[:, 4 * HEAD_WIDTH : 5 * HEAD_WIDTH]
-        yield
-        up.arrive()
-        rows = head_columns(xm, core, 0)
-        far_up = send(rows, rows, x_plus)
-        rows = head_columns(xm, core)
-        out_swap.append(send(rows, rows, partner))
-        down.arrive()
-        rows = head_columns(xp, core, 1)
-        far_down = send(rows, rows, x_minus)
-        rows = head_columns(xp, core)
-        out_swap.append(send(rows, rows, partner))
-        yield
-        far_up.arrive()
-        rows = head_columns(turn(x, 2), core, 0)
-        out_swap.append(send(rows, rows, partner))
-        far_down.arrive()
-        rows = head_columns(turn(x, 2), core, 1)
-        out_swap.append(send(rows, rows, partner))
-        yield
-
-    steps["o"] = out_steps()
-
-    go("00t1t0t1t0t10t100tt")
-    keys_of(0)
-    pass_all(0)
-    go("1to11")
-    keys_of(-1)
-    pass_all(-1)
-    keys_of(1)
-    pass_all(1)
-    go("ttt")
-    keys_of(2)
-    for b in range(SHARE):
-        for keys, group in ((wide, 2), (middle, 1)):
-            pass_on(keys, group, turn(x, 2), pl.ds(b, 1))
-    go("1")
-
     def keys_near(x_at, carry):
         found = project(x_at, UNITS[1][0], 2 * HEAD_WIDTH)
         for which in (0, 1):
             lay(found, which * HEAD_WIDTH, near.at[which], x_at, AHEAD[0])
         return carry
-
-    lax.fori_loop(0, 4, keys_near, 0)
-    near_halo = send(near.at[:, :, BLOCKS, 96:, :], near.at[:, :, 0, 96:, :], later)
 
     def ask(x_at, carry):
         left = UNITS[1][0] + 2 * HEAD_WIDTH
@@ -440,7 +449,31 @@
         lay(project(x_at, left + 2 * HEAD_WIDTH, HEAD_WIDTH), 0, queries.at[0], x_at, 0)
         return carry
 
-    lax.fori_loop(0, 4, ask, 0)
+    def early_keys(step):
+        keys_of(step)
+        pass_all(step)
+
+    for letter, step in (("0", 0), ("m", -1), ("p", 1)):
+        events["K" + letter] = functools.partial(early_keys, step)
+
+    @out_event("K2")
+    def _():
+        keys_of(2)
+        for b in range(SHARE):
+            for keys, group in ((wide, 2), (middle, 1)):
+                pass_on(keys, group, turn(x, 2), pl.ds(b, 1))
+
+    @out_event("N")
+    def _():
+        lax.fori_loop(0, 4, keys_near, 0)
+        halo.append(send(near.at[:, :, BLOCKS, 96:, :], near.at[:, :, 0, 96:, :], later))
+
+    @out_event("Q")
+    def _():
+        lax.fori_loop(0, 4, ask, 0)
+
+    for name in ORDER:
+        events[name]()
 
     factor = math.log2(math.e) / math.sqrt(HEAD_WIDTH)
     start_at = (z * 2 + upper) * ROWS
@@ -477,9 +510,9 @@
 
     for b in range(SHARE):
         attend(b, BLOCKS - 1)
-    go("o")
-    near_halo.arrive()
-    for copy in halo[:6]:
+    events["ofu"]()
+    events["ofd"]()
+    for copy in halo[:6] + halo[12:]:
         copy.arrive()
     exchange = Transfer()
     for b in range(SHARE):
@@ -501,8 +534,6 @@
                     log_rows.at[line_at * 2 + core_at], both_logs.at[core, share], device
                 )
         arrived[share * SHARE + b, :, lanes] = combined[b, rows_for(line, core, x), :]
-        if b == 0:
-            go("o")
     both_logs[core, share] = log_rows[line * 2 + core]
     for copy in out_swap + [exchange]:
         copy.arrive()

time: 83.5 us -> 79 us (0.946)
  Pallas kernels: 81.3 us -> 76.7 us
    pallas_call x1, Pallas kernels: 81.3 us -> 76.7 us  [shards(): pl.pallas_call(kernel, out_shape=(jax.ShapeDtypeStruct((BATCH, 32, WIDTH)...]
where the time goes in v4:
time: 79 us; the launch traced here: 78.8 us
  Pallas kernels  76.7 us (97%)
  local copies, waits for them, and re-layouts  1.47 us (2%)
    pallas_call x1, Pallas kernels, shards(): pl.pallas_call(kernel, out_shape=(jax.ShapeDtypeStruct((BATCH, 32, WIDTH)...  76.7 us

profile of v4, /device:TPU:1, one launch (start us, length us, event | category | flops | bytes accessed | tf_op | source)
XLA Modules:
  0.0 78.8 jit_solution(15888271549969706283)
XLA Ops:
  0.6 76.7 %shard_map.77 = (bf16[6,32,2048]{2,1,0:T(8,128)(2,1)S(1)}, f32[6,2,128]{2,1,0:T(2,128)S(1)}) custom-call(bf16[6,32,2048]{2,1,0:T(8,128)(2,1)} %bitcast.7, f32[1,2048]{1,0:T(1,128)} %bitcast.9, bf16[3,64,256]{2,1,0:T(8,128)(2,1)} %w_query.1, bf16[3,64,256]{2,1,0:T(8,128)(2,1)} %w_key.1, bf16[3,64,256]{2,1,0:T(8,128)(2,1)} %w_value.1, bf16[64,256]{1,0:T(8,128)(2,1)} %bitcast.8), custom_call_target="tpu_custom_call" | custom-call | tf_op jit(solution)/shard_map/pallas_call | solution.py:566
  77.4 0.9 %copy.10 = bf16[32,6,2048]{2,0,1:T(8,128)(2,1)} copy(bf16[32,6,2048]{2,0,1:T(8,128)(2,1)S(1)} %bitcast.5) | data formatting | bytes 1572864
  78.2 0.6 copy.11

commit v5 on v4

--- a/solution.py
+++ b/solution.py
@@ -34,11 +34,11 @@
     "g2", "Zm01", "Zp01", "Oa1", "Ypm0", "up10", "dn11", "Yaf0", "Ypp0", "Rm1", "fu1", "Rp1",
     "fd0", "Zmf0", "Zpf0", "Op1", "Ya01", "Ypf0", "fu2", "dn12", "Zma1", "Zpa1", "Yp01",
     "Rf1", "Yam1", "up11", "fd1", "Of1", "Yap1", "Zmp1", "Zpp1", "Ypm1", "W0", "o0", "K0",
-    "up12", "fd2", "Ypp1", "Yaf1", "Zmf1", "Zpf1", "Km", "Ypf1", "Kp", "K2", "W1", "N", "oum",
-    "odm", "Q",
+    "up12", "fd2", "Ypp1", "Yaf1", "Zmf1", "Zpf1", "Km", "Ypf1", "Kp", "K2", "oum", "odm",
+    "W1", "N", "Q",
 )
-Y_CUT = (0, 64)
-Z_CUT = (32, 32)
+Y_CUT = (16, 64)
+Z_CUT = (48, 48)
 
 epsilon = 1e-06
 MESH = pl.DeviceIdType.MESH
@@ -510,8 +510,6 @@
 
     for b in range(SHARE):
         attend(b, BLOCKS - 1)
-    events["ofu"]()
-    events["ofd"]()
     for copy in halo[:6] + halo[12:]:
         copy.arrive()
     exchange = Transfer()
@@ -535,6 +533,8 @@
                 )
         arrived[share * SHARE + b, :, lanes] = combined[b, rows_for(line, core, x), :]
     both_logs[core, share] = log_rows[line * 2 + core]
+    events["ofu"]()
+    events["ofd"]()
     for copy in out_swap + [exchange]:
         copy.arrive()
 

time: 79 us -> 71.2 us (0.901)
  Pallas kernels: 76.7 us -> 68.9 us
    pallas_call x1, Pallas kernels: 76.7 us -> 68.9 us  [shards(): pl.pallas_call(kernel, out_shape=(jax.ShapeDtypeStruct((BATCH, 32, WIDTH)...]
where the time goes in v5:
time: 71.2 us; the launch traced here: 71 us
  Pallas kernels  68.9 us (97%)
  local copies, waits for them, and re-layouts  1.47 us (2%)
    pallas_call x1, Pallas kernels, shards(): pl.pallas_call(kernel, out_shape=(jax.ShapeDtypeStruct((BATCH, 32, WIDTH)...  68.9 us
    unnamed x2, local copies, waits for them, and re-layouts  1.47 us

profile of v5, /device:TPU:1, one launch (start us, length us, event | category | flops | bytes accessed | tf_op | source)
XLA Modules:
  0.0 71.0 jit_solution(7060870657183461025)
XLA Ops:
  0.6 68.9 %shard_map.77 = (bf16[6,32,2048]{2,1,0:T(8,128)(2,1)S(1)}, f32[6,2,128]{2,1,0:T(2,128)S(1)}) custom-call(bf16[6,32,2048]{2,1,0:T(8,128)(2,1)} %bitcast.7, f32[1,2048]{1,0:T(1,128)} %bitcast.9, bf16[3,64,256]{2,1,0:T(8,128)(2,1)} %w_query.1, bf16[3,64,256]{2,1,0:T(8,128)(2,1)} %w_key.1, bf16[3,64,256]{2,1,0:T(8,128)(2,1)} %w_value.1, bf16[64,256]{1,0:T(8,128)(2,1)} %bitcast.8), custom_call_target="tpu_custom_call" | custom-call | tf_op jit(solution)/shard_map/pallas_call | solution.py:566
  69.5 0.9 %copy.10 = bf16[32,6,2048]{2,0,1:T(8,128)(2,1)} copy(bf16[32,6,2048]{2,0,1:T(8,128)(2,1)S(1)} %bitcast.5) | data formatting | bytes 1572864
  70.4 0.6 copy.11

commit v6 on v5

--- a/solution.py
+++ b/solution.py
@@ -193,23 +193,22 @@
             along_y = names[0] == "pair"
             self.from_first = to_first if along_y else to_second
             self.from_second = to_second if along_y else to_first
-            self.on = []
+            self.on = Transfer()
 
         def pass_first(self):
             self.from_first.arrive()
             if self.cut < PIECE:
                 rows = self.rows_of(self.names[0], self.cut, PIECE - self.cut)
-                self.on.append(send(rows, rows, self.second))
+                self.on.begin(rows, rows, self.second)
 
         def pass_second(self):
             self.from_second.arrive()
             if self.cut > 0:
                 rows = self.rows_of(self.names[1], 0, self.cut)
-                self.on.append(send(rows, rows, self.first))
+                self.on.begin(rows, rows, self.first)
 
         def far(self):
-            for copy in self.on:
-                copy.arrive()
+            self.on.arrive()
 
     ys = {0: y, "pair": pair_y, "apart": apart_y, "far": turn(y, 2)}
     zs = {0: z, -1: zm, 1: zp, 2: turn(z, 2)}
@@ -378,7 +377,7 @@
             return whole_out.at[:, lanes]
         return whole_out.at[pl.ds(half * (WIDTH // 2), WIDTH // 2), lanes]
 
-    out_swap = []
+    out_swap = Transfer()
 
     out_way = {}
 
@@ -388,7 +387,7 @@
         return keep
 
     def out_cross(rows):
-        out_swap.append(send(rows, rows, partner))
+        out_swap.begin(rows, rows, partner)
 
     @out_event("o0")
     def _():
@@ -396,7 +395,7 @@
         mine = head_columns(x, core)
         out_way["up"] = send(out_rows, mine, x_plus)
         out_way["down"] = send(out_rows, mine, x_minus)
-        out_swap.append(send(out_rows, mine, partner))
+        out_swap.begin(out_rows, mine, partner)
         lanes = pl.ds(pl.multiple_of(head * HEAD_WIDTH, HEAD_WIDTH), HEAD_WIDTH)
         whole_out[:, lanes] = weights[:, 4 * HEAD_WIDTH : 5 * HEAD_WIDTH]
 
@@ -535,8 +534,8 @@
     both_logs[core, share] = log_rows[line * 2 + core]
     events["ofu"]()
     events["ofd"]()
-    for copy in out_swap + [exchange]:
-        copy.arrive()
+    out_swap.arrive()
+    exchange.arrive()
 
     everything = arrived[...].reshape(192, HEADS * HEAD_WIDTH)
     for tile in range(8):
@@ -553,7 +552,7 @@
         pltpu.make_async_copy(whole, whole, send_sem.at[index]).wait()
 
 
-ARRIVALS = 130
+ARRIVALS = 106
 SENDS = 8
 
 

time: 71.2 us -> 70.9 us (level)
  no operation moved by 1% of the time
where the time goes in v6:
time: 70.9 us; the launch traced here: 70.8 us
  Pallas kernels  68.7 us (97%)
  local copies, waits for them, and re-layouts  1.47 us (2%)
    pallas_call x1, Pallas kernels, shards(): pl.pallas_call(kernel, out_shape=(jax.ShapeDtypeStruct((BATCH, 32, WIDTH)...  68.7 us
    unnamed x2, local copies, waits for them, and re-layouts  1.47 us

profile of v6, /device:TPU:1, one launch (start us, length us, event | category | flops | bytes accessed | tf_op | source)
XLA Modules:
  0.0 70.8 jit_solution(15641972783786810911)
XLA Ops:
  0.6 68.7 %shard_map.77 = (bf16[6,32,2048]{2,1,0:T(8,128)(2,1)S(1)}, f32[6,2,128]{2,1,0:T(2,128)S(1)}) custom-call(bf16[6,32,2048]{2,1,0:T(8,128)(2,1)} %bitcast.7, f32[1,2048]{1,0:T(1,128)} %bitcast.9, bf16[3,64,256]{2,1,0:T(8,128)(2,1)} %w_query.1, bf16[3,64,256]{2,1,0:T(8,128)(2,1)} %w_key.1, bf16[3,64,256]{2,1,0:T(8,128)(2,1)} %w_value.1, bf16[64,256]{1,0:T(8,128)(2,1)} %bitcast.8), custom_call_target="tpu_custom_call" | custom-call | tf_op jit(solution)/shard_map/pallas_call | solution.py:565
  69.3 0.9 %copy.10 = bf16[32,6,2048]{2,0,1:T(8,128)(2,1)} copy(bf16[32,6,2048]{2,0,1:T(8,128)(2,1)S(1)} %bitcast.5) | data formatting | bytes 1572864
  70.2 0.6 copy.11
